TPU v7x, 1024 devices: a whole 8x8x8 slice. The times are simulated.
1024 devices in a mesh: ep: 64 (over z, y), tp: 16 (over x, core).
Axes of the slice: x: 8, y: 8, z: 8, core: 2. Of those that a mesh axis runs over, the one named last changes fastest.
Arguments:
- tokens: bfloat16 [16384, 2048], P('ep', 'tp'), may hold values from -6 to 6
- experts: int32 [16384, 16], P('ep'), may hold values from 0 to 262143, as said below
- weights: float32 [16384, 16], P('ep'), may hold values from 0.05 to 1
- up_table: bfloat16 [262144, 2048], P('ep', 'tp'), may hold values from -0.125 to 0.125
- out_table: bfloat16 [262144, 2048], P('ep', 'tp')
- gain: float32 [2048], P('tp'), may hold values from 0.1 to 1.9
Outputs:
- normed: bfloat16 [16384, 2048], P('ep', 'tp')
Inputs may be any that keep to these rules, and one draw needn't show every extreme that they name: An expert number e lies with index e // 4096 of ep. Among the rows of one index of ep, at most 128 chosen experts lie with any one index of ep, and in every draw some index of ep receives exactly 128 from every index.
All inputs are finite; a program needn't handle non-finite values.
Results may differ from a plain program's by a relative error of at most 0.006.
Values may be sent and summed in bfloat16 or wider, within the bound.
A program may use at most 32 MiB of HBM per device.

v0:
```python
import jax
import jax.numpy as jnp
from jax import lax
from jax.sharding import PartitionSpec as P


def gathered_total(array, axis):
    return lax.all_gather(array, axis).sum(0)


def from_everyone(array, axis):
    copies = jnp.broadcast_to(array, (lax.axis_size(axis), *array.shape))
    return lax.all_to_all(copies, axis, split_axis=0, concat_axis=0, tiled=True)


def of_everyone(array, axis):
    everything = from_everyone(array, axis)
    return jnp.sum(everything, axis=0)


def owner_ranks(owner, n_ep):
    request_list = owner.shape[0]
    block_len = 512
    block_count = request_list // block_len
    onehot = (owner[:, None] == jnp.arange(n_ep, dtype=jnp.int32)[None, :]).astype(jnp.bfloat16)
    onehot_blocks = onehot.reshape(block_count, block_len, n_ep)
    row_pos = jnp.arange(block_len, dtype=jnp.int32)
    lower = (row_pos[:, None] >= row_pos[None, :]).astype(jnp.bfloat16)
    within = jnp.einsum("ij,bjn->bin", lower, onehot_blocks, preferred_element_type=jnp.float32)
    totals = within[:, block_len - 1, :]
    before = jnp.cumsum(totals, axis=0) - totals
    counted = jnp.sum((within + before[:, None, :]) * onehot_blocks.astype(jnp.float32), axis=2)
    return counted.reshape(request_list).astype(jnp.int32) - 1


def body(tokens, experts, weights, up_table, out_table, gain):
    n_ep = lax.axis_size("ep")
    tok_rows, width = tokens.shape
    slots = experts.shape[1]
    rows_held = up_table.shape[0]
    request_list = tok_rows * slots
    capacity = 2 * request_list // n_ep
    flat = experts.reshape(-1)
    owner = flat // rows_held
    local_row = flat - owner * rows_held
    rank = owner_ranks(owner, n_ep)
    position = owner * capacity + rank
    send_ids = (
        jnp.zeros((n_ep * capacity,), jnp.int32).at[position].set(local_row).reshape(n_ep, capacity)
    )
    source = (
        jnp.full((n_ep * capacity,), -1, jnp.int32)
        .at[position]
        .set(jnp.arange(request_list, dtype=jnp.int32))
    )
    filled = source >= 0
    token_of = jnp.maximum(source, 0) // slots
    picked = jnp.take(tokens, token_of, axis=0)
    send_feat = jnp.where(filled[:, None], picked, jnp.zeros_like(picked)).reshape(
        n_ep, capacity, width
    )
    feat = lax.all_to_all(send_feat, "ep", split_axis=0, concat_axis=0, tiled=True)
    ids = lax.all_to_all(send_ids, "ep", split_axis=0, concat_axis=0, tiled=True)
    partial_value = jnp.einsum(
        "scw,scw->sc", feat, up_table[ids], preferred_element_type=jnp.float32
    )
    dot = gathered_total(partial_value, "tp")
    act = jax.nn.gelu(dot)
    contrib = (act[:, :, None] * out_table[ids]).astype(jnp.bfloat16)
    back = lax.all_to_all(contrib, "ep", split_axis=0, concat_axis=0, tiled=True)
    contrib = jnp.take(back.reshape(n_ep * capacity, width), position, axis=0).reshape(
        tok_rows, slots, width
    )
    mixed = jnp.einsum("tk,tkw->tw", weights, contrib.astype(jnp.float32))
    square = of_everyone(jnp.sum(mixed * mixed, axis=1), "tp")
    scale = lax.rsqrt(square / (width * lax.axis_size("tp")) + 1e-06)
    return (mixed * scale[:, None] * gain[None, :]).astype(jnp.bfloat16)


def solution(mesh):
    placed = (P("ep", "tp"), P("ep", None), P("ep", None), P("ep", "tp"), P("ep", "tp"), P("tp"))
    return jax.shard_map(body, mesh=mesh, in_specs=placed, out_specs=P("ep", "tp"), check_vma=False)
```

profile of v0, /device:TPU:1, one launch (start us, length us, event | category | flops | bytes accessed | tf_op | source)
XLA Modules:
  0.0 281.5 jit_solution(5360069832734767673)
XLA Ops:
  0.0 0.0 copy-start
  0.0 0.0 copy-start.1
  0.0 0.9 copy.30
  0.9 0.1 reshape.230
  1.0 0.1 reshape.231
  1.1 0.1 reshape.232
  1.3 0.5 convolution_bitcast_fusion
  1.8 0.3 fusion.37
  2.1 0.3 multiply_reduce_fusion
  2.4 0.1 compare_select_fusion
  2.5 16.1 %scatter_custom_fusion.1 = s32[8192]{0:T(1024)} fusion(s32[4096]{0:T(1024)S(1)} %bitcast.41, s32[4096]{0:T(1024)S(1)} %fusion.27, s32[]{:T(128)} %constant.46.clone.1), kind=kCustom, calls=%fused_computation.71 | custom fusion | bytes 32772 | tf_op jit(solution)/shard_map/scatter | solution.py:49
  18.6 23.9 %all-to-all-start.1 = ((s32[64,1,128]{2,1,0:T(1,128)}), s32[64,1,128]{2,1,0:T(1,128)S(1)}, u32[]{:S(2)}, u32[]{:S(2)}) async-start(s32[64,1,128]{2,1,0:T(1,128)} %bitcast.6), calls=%async_computation.1 | async-start | bytes 65536 | tf_op jit(solution)/shard_map/all_to_all | solution.py:63
  42.6 15.5 %scatter_custom_fusion = s32[8192]{0:T(1024)S(1)} fusion(s32[4096]{0:T(1024)S(1)} %bitcast.42, s32[4096]{0:T(1024)S(1)} %iota.21, s32[]{:T(128)} %constant.74.clone.1), kind=kCustom, calls=%fused_computation.73 | custom fusion | bytes 32772 | tf_op jit(solution)/shard_map/scatter | solution.py:54
  58.2 0.0 copy-done.1
  58.2 24.0 %gather_fusion = bf16[8192,128]{1,0:T(8,128)(2,1)S(1)} fusion(bf16[256,128]{1,0:T(8,128)(2,1)S(1)} %copy-done.1, s32[8192]{0:T(1024)S(1)} %broadcast_clamp_fusion), kind=kCustom, calls=%fused_computation | custom fusion | bytes 4227072 | tf_op jit(solution)/shard_map/jit(_take)/gather | solution.py:58
  82.3 4.6 %select_select_fusion = bf16[64,128,128]{2,1,0:T(8,128)(2,1)} fusion(bf16[64,128,128]{2,1,0:T(8,128)(2,1)S(1)} %bitcast.35, pred[64,128]{1,0:T(8,128)(4,1)S(1)} %get-tuple-element.6, pred[64,128]{1,0:T(8,128)(4,1)S(1)} %get-tuple-element.5), kind=kLoop, calls=%fused_computation.10 | loop fusion | flops 2097152 | bytes 4210688 | tf_op jit(solution)/shard_map/jit(_where)/select_n | solution.py:59
  86.8 0.0 all-to-all-done.1
  86.9 12.4 %all-to-all-start = ((bf16[64,128,128]{2,1,0:T(8,128)(2,1)}), bf16[64,128,128]{2,1,0:T(8,128)(2,1)}, u32[]{:S(2)}, u32[]{:S(2)}) async-start(bf16[64,128,128]{2,1,0:T(8,128)(2,1)} %select_select_fusion), calls=%async_computation | async-start | bytes 4194304 | tf_op jit(solution)/shard_map/all_to_all | solution.py:62
  99.3 0.0 copy-done
  99.3 0.0 copy-start.2
  99.3 29.2 %gather_fusion.1 = bf16[8192,128]{1,0:T(8,128)(2,1)} fusion(bf16[4096,128]{1,0:T(8,128)(2,1)S(1)} %copy-done, s32[8192]{0:T(1024)S(1)} %fusion.19), kind=kCustom, calls=%fused_computation.1 | custom fusion | bytes 4227072 | tf_op jit(solution)/shard_map/gather | solution.py:65
  128.5 0.0 copy-done.2
  128.5 29.2 %gather_fusion.2 = bf16[8192,128]{1,0:T(8,128)(2,1)} fusion(bf16[4096,128]{1,0:T(8,128)(2,1)S(1)} %copy-done.2, s32[8192]{0:T(1024)S(1)} %fusion.19), kind=kCustom, calls=%fused_computation.2 | custom fusion | bytes 4227072 | tf_op jit(solution)/shard_map/gather | solution.py:69
  157.7 0.0 all-to-all-done
  157.7 0.0 copy-start.3
  157.7 3.5 %fusion.1 = f32[64,128]{1,0:T(8,128)S(1)} fusion(bf16[64,128,128]{2,1,0:T(8,128)(2,1)} %all-to-all-done, bf16[64,128,128]{2,1,0:T(8,128)(2,1)} %bitcast.34), kind=kLoop, calls=%fused_computation.9 | loop fusion | flops 4186112 | bytes 4227072 | tf_op jit(solution)/shard_map/scw,scw->sc/dot_general | solution.py:64
  161.3 21.2 %all-gather = f32[1024,128]{1,0:T(8,128)} all-gather(f32[64,128]{1,0:T(8,128)S(1)} %fusion.1), channel_id=2, replica_groups=mesh['ep'=64,'tp'=16] {'tp'}, dimensions={0}, use_global_device_ids=true | all-gather | bytes 557056 | tf_op jit(solution)/shard_map/all_gather | solution.py:8
  182.4 1.1 reduce_sum.37
  183.6 0.0 copy-done.3
  183.6 2.3 fusion
  185.9 0.0 copy-start.4
  185.9 0.0 copy-start.5
  185.9 12.5 %all-to-all-start.2 = ((bf16[64,128,128]{2,1,0:T(8,128)(2,1)}), bf16[64,128,128]{2,1,0:T(8,128)(2,1)S(1)}, u32[]{:S(2)}, u32[]{:S(2)}) async-start(bf16[64,128,128]{2,1,0:T(8,128)(2,1)} %fusion), calls=%async_computation.2 | async-start | bytes 4194304 | tf_op jit(solution)/shard_map/all_to_all | solution.py:70
  198.4 0.1 sub.37
  198.5 0.1 copy.31
  198.5 0.0 copy-done.4
  198.6 0.1 copy.32
  198.7 0.0 copy-done.5
  198.7 0.1 copy.40
  198.9 49.6 %all-to-all-done.2 = bf16[64,128,128]{2,1,0:T(8,128)(2,1)S(1)} async-done(((bf16[64,128,128]{2,1,0:T(8,128)(2,1)}), bf16[64,128,128]{2,1,0:T(8,128)(2,1)S(1)}, u32[]{:S(2)}, u32[]{:S(2)}) %all-to-all-start.2) | async-done | bytes 2097184 | tf_op jit(solution)/shard_map/all_to_all | solution.py:70
  248.4 14.9 %gather_fusion.3 = bf16[4096,128]{1,0:T(8,128)(2,1)} fusion(bf16[8192,128]{1,0:T(8,128)(2,1)S(1)} %bitcast.32, s32[4096]{0:T(1024)S(1)} %broadcast_clamp_fusion.1), kind=kCustom, calls=%fused_computation.3 | custom fusion | bytes 2113536 | tf_op jit(solution)/shard_map/jit(_take)/gather | solution.py:71
  263.3 0.0 copy-start.6
  263.3 2.0 fusion.2
  265.3 0.1 multiply_reduce_fusion.1
  265.4 15.3 %all_to_all.28 = f32[16,1,256]{2,1,0:T(1,128)S(1)} all-to-all(f32[16,1,256]{2,1,0:T(1,128)S(1)} %broadcast_in_dim.66), channel_id=1, replica_groups=mesh['ep'=64,'tp'=16] {'tp'}, dimensions={0} | all-to-all | bytes 32768 | tf_op jit(solution)/shard_map/all_to_all | solution.py:13
  280.7 0.0 copy-done.6
  280.7 0.7 multiply_convert_fusion
  (14 shorter events, 0.2 us)
Async XLA Ops:
  0.0 99.3 %copy-start = (bf16[4096,128]{1,0:T(8,128)(2,1)S(1)}, bf16[4096,128]{1,0:T(8,128)(2,1)}, u32[]{:S(2)}) copy-start(bf16[4096,128]{1,0:T(8,128)(2,1)} %param.9) | copy-start | bytes 3145732
  0.0 58.2 %copy-start.1 = (bf16[256,128]{1,0:T(8,128)(2,1)S(1)}, bf16[256,128]{1,0:T(8,128)(2,1)}, u32[]{:S(2)}) copy-start(bf16[256,128]{1,0:T(8,128)(2,1)} %param.6) | copy-start | bytes 196612
  18.6 68.2 %all-to-all-start.1 = ((s32[64,1,128]{2,1,0:T(1,128)}), s32[64,1,128]{2,1,0:T(1,128)S(1)}, u32[]{:S(2)}, u32[]{:S(2)}) async-start(s32[64,1,128]{2,1,0:T(1,128)} %bitcast.6), calls=%async_computation.1 | async-start | bytes 65536 | tf_op jit(solution)/shard_map/all_to_all | solution.py:63
  86.9 70.9 %all-to-all-start = ((bf16[64,128,128]{2,1,0:T(8,128)(2,1)}), bf16[64,128,128]{2,1,0:T(8,128)(2,1)}, u32[]{:S(2)}, u32[]{:S(2)}) async-start(bf16[64,128,128]{2,1,0:T(8,128)(2,1)} %select_select_fusion), calls=%async_computation | async-start | bytes 4194304 | tf_op jit(solution)/shard_map/all_to_all | solution.py:62
  99.3 29.2 %copy-start.2 = (bf16[4096,128]{1,0:T(8,128)(2,1)S(1)}, bf16[4096,128]{1,0:T(8,128)(2,1)}, u32[]{:S(2)}) copy-start(bf16[4096,128]{1,0:T(8,128)(2,1)} %param.10) | copy-start | bytes 3145732
  157.7 25.8 %copy-start.3 = (bf16[8192,128]{1,0:T(8,128)(2,1)S(1)}, bf16[8192,128]{1,0:T(8,128)(2,1)}, u32[]{:S(2)}) copy-start(bf16[8192,128]{1,0:T(8,128)(2,1)} %gather_fusion.2) | copy-start | bytes 6291460
  185.9 12.7 %copy-start.4 = (s32[256,16]{0,1:T(8,128)S(1)}, s32[256,16]{0,1:T(8,128)}, u32[]{:S(2)}) copy-start(s32[256,16]{0,1:T(8,128)} %param.7) | copy-start | bytes 49156
  185.9 12.8 %copy-start.5 = (f32[256,16]{0,1:T(8,128)S(1)}, f32[256,16]{0,1:T(8,128)}, u32[]{:S(2)}) copy-start(f32[256,16]{0,1:T(8,128)} %param.8) | copy-start | bytes 49156
  185.9 62.6 %all-to-all-start.2 = ((bf16[64,128,128]{2,1,0:T(8,128)(2,1)}), bf16[64,128,128]{2,1,0:T(8,128)(2,1)S(1)}, u32[]{:S(2)}, u32[]{:S(2)}) async-start(bf16[64,128,128]{2,1,0:T(8,128)(2,1)} %fusion), calls=%async_computation.2 | async-start | bytes 4194304 | tf_op jit(solution)/shard_map/all_to_all | solution.py:70
  263.3 17.4 %copy-start.6 = (f32[128]{0:T(128)S(1)}, f32[128]{0:T(128)}, u32[]{:S(2)}) copy-start(f32[128]{0:T(128)} %param.11) | copy-start | bytes 1540
where the time goes:
time: 282 us; the launch traced here: 281 us
  local copies, waits for them, and re-layouts  131 us (46%)
  waiting for transfers between devices  49.6 us (18%)
  starting transfers between devices  48.8 us (17%)
  blocking collectives  36.4 us (13%)
  other arithmetic  13.2 us (5%)
    all_to_all x1, waiting for transfers between devices, body(): lax.all_to_all(contrib, 'ep', split_axis=0, concat_axis=0, tiled=True)  49.6 us
    gather x1, local copies, waits for them, and re-layouts, body(): contrib = (act[:, :, None] * out_table[ids]).astype(jnp.bfloat16)  29.2 us
    gather x1, local copies, waits for them, and re-layouts, body(): up_table[ids]  29.2 us
    gather x1, local copies, waits for them, and re-layouts, body(): picked = jnp.take(tokens, token_of, axis=0)  24 us
    all_to_all x1, starting transfers between devices, body(): lax.all_to_all(send_ids, 'ep', split_axis=0, concat_axis=0, tiled=True)  23.9 us
    all_gather x1, blocking collectives, gathered_total(): return lax.all_gather(array, axis).sum(0)  21.2 us
    scatter x1, local copies, waits for them, and re-layouts, body(): jnp.zeros((n_ep * capacity,), jnp.int32).at[position].set(local_row)  16.1 us
    scatter x1, local copies, waits for them, and re-layouts, body(): source = jnp.full((n_ep * capacity,), -1, jnp.int32).at[position].set(jnp...  15.5 us
  transfers between devices with their start and end apart: 3, of which 1 were waited for; matrix products, arithmetic and copies ran while one was open for 37% of the time, Pallas kernels for 0%

commit v1 on v0

v1 whole, which is shorter than its diff:
```python
import functools

import jax
import jax.numpy as jnp
from jax import lax
from jax.experimental import pallas as pl
from jax.experimental.pallas import tpu as pltpu
from jax.sharding import PartitionSpec as P

F32, BF16, I32 = jnp.float32, jnp.bfloat16, jnp.int32
CONTRACT_MINOR = (((1,), (1,)), ((), ()))


def bucket_kernel(rows_held, expert_ref, weight_ref, id_ref, tok_ref, wgt_ref):
    slots, toks = expert_ref.shape
    owners, cap = id_ref.shape
    shift = rows_held.bit_length() - 1
    owner_no = lax.broadcasted_iota(I32, (owners, toks), 0)
    rank_no = lax.broadcasted_iota(I32, (cap, toks), 0)
    token_no = lax.broadcasted_iota(I32, (1, toks), 1).astype(F32)
    first = lax.broadcasted_iota(I32, (toks, toks), 0)
    second = lax.broadcasted_iota(I32, (toks, toks), 1)
    earlier = jnp.where(first < second, 1.0, 0.0).astype(BF16)
    ones = jnp.ones((toks, toks), BF16)
    before = jnp.zeros((owners, toks), F32)
    found = jnp.zeros((5 * owners, cap), F32)
    for k in range(slots):
        expert = expert_ref[k : k + 1, :]
        local = expert & (rows_held - 1)
        mine = (expert >> shift) == owner_no
        onehot = jnp.where(mine, 1.0, 0.0).astype(BF16)
        rank = before + jnp.dot(onehot, earlier, preferred_element_type=F32)
        before = before + jnp.dot(onehot, ones, preferred_element_type=F32)
        rank = jnp.sum(jnp.where(mine, rank, 0.0), axis=0, keepdims=True).astype(I32)
        place = jnp.where(rank == rank_no, 1.0, 0.0).astype(BF16)
        weight = weight_ref[k : k + 1, :]
        weight_hi = weight.astype(BF16).astype(F32)
        pieces = (
            (local >> 8).astype(F32),
            (local & 255).astype(F32),
            token_no,
            weight_hi,
            weight - weight_hi,
        )
        what = jnp.concatenate([jnp.where(mine, p, 0.0).astype(BF16) for p in pieces], axis=0)
        found = found + lax.dot_general(what, place, CONTRACT_MINOR, preferred_element_type=F32)
    part = [found[i * owners : (i + 1) * owners] for i in range(5)]
    id_ref[...] = (part[0] * 256.0 + part[1]).astype(I32)
    tok_ref[...] = part[2]
    wgt_ref[...] = part[3] + part[4]


def dots_kernel(id_ref, tok_ref, feat_ref, up_ref, out_ref, dot_ref, rows_ref, table, pair):
    step = pl.program_id(0)
    held = up_ref.shape[0]
    cap = id_ref.shape[1]
    toks = feat_ref.shape[1]

    @pl.when(step == 0)
    def _():
        table[pl.ds(0, held, stride=2), :] = up_ref[...].astype(F32)
        table[pl.ds(1, held, stride=2), :] = out_ref[...].astype(F32)

    for r in range(cap):
        row = id_ref[step, r]
        pair[2 * r : 2 * r + 2, :] = table[pl.ds(pl.multiple_of(row * 2, 2), 2), :]
    up = pair[pl.ds(0, cap, stride=2), :].astype(BF16)
    rows_ref[0] = pair[pl.ds(1, cap, stride=2), :].astype(BF16)
    every = lax.dot_general(feat_ref[0], up, CONTRACT_MINOR, preferred_element_type=F32)
    token = lax.broadcasted_iota(I32, (toks, cap), 0).astype(F32)
    dot_ref[0] = jnp.sum(jnp.where(tok_ref[0] == token, every, 0.0), axis=0, keepdims=True)


def mix_kernel(tok_ref, wgt_ref, dot_ref, rows_ref, mixed_ref):
    toks = mixed_ref.shape[1]
    cap = tok_ref.shape[2]
    coef = jax.nn.gelu(dot_ref[0]) * wgt_ref[0]
    coef_hi = coef.astype(BF16).astype(F32)
    token = lax.broadcasted_iota(I32, (toks, cap), 0).astype(F32)
    here = tok_ref[0] == token
    spread = jnp.concatenate(
        [jnp.where(here, c, 0.0).astype(BF16) for c in (coef_hi, coef - coef_hi)], axis=1
    )
    rows = jnp.concatenate([rows_ref[0]] * 2, axis=0)
    mixed_ref[0] = jnp.dot(spread, rows, preferred_element_type=F32).astype(mixed_ref.dtype)


def body(tokens, experts, weights, up_table, out_table, gain):
    n_ep, n_tp = lax.axis_size("ep"), lax.axis_size("tp")
    toks, width = tokens.shape
    slots = experts.shape[1]
    held = up_table.shape[0]
    cap = 2 * toks * slots // n_ep
    listed = jax.ShapeDtypeStruct((n_ep, cap), F32)
    ids, tok, wgt = pl.pallas_call(
        functools.partial(bucket_kernel, held),
        out_shape=(jax.ShapeDtypeStruct((n_ep, cap), I32), listed, listed),
        name="bucket",
    )(experts.T, weights.T)
    exchange = functools.partial(
        lax.all_to_all, axis_name="ep", split_axis=0, concat_axis=0, tiled=True
    )
    ids = exchange(ids)
    tokwgt = exchange(jnp.stack([tok, wgt], axis=1))
    feat = lax.all_gather(tokens, "ep")
    tok, wgt = tokwgt[:, :1], tokwgt[:, 1:]
    lane = pl.BlockSpec((1, 1, cap), lambda s, *_: (s, 0, 0))
    whole = pl.BlockSpec((held, width), lambda s, *_: (0, 0))
    block = pl.BlockSpec((1, toks, width), lambda s, *_: (s, 0, 0))
    rows = pl.BlockSpec((1, cap, width), lambda s, *_: (s, 0, 0))
    dot, picked = pl.pallas_call(
        dots_kernel,
        grid_spec=pltpu.PrefetchScalarGridSpec(
            num_scalar_prefetch=1,
            grid=(n_ep,),
            in_specs=[lane, block, whole, whole],
            out_specs=[lane, rows],
            scratch_shapes=[pltpu.VMEM((2 * held, width), F32), pltpu.VMEM((2 * cap, width), F32)],
        ),
        out_shape=(
            jax.ShapeDtypeStruct((n_ep, 1, cap), F32),
            jax.ShapeDtypeStruct((n_ep, cap, width), BF16),
        ),
        name="dots",
    )(ids, tok, feat, up_table, out_table)
    dot = lax.psum(dot, "tp")
    mixed = pl.pallas_call(
        mix_kernel,
        grid=(n_ep,),
        in_specs=[lane, lane, lane, rows],
        out_specs=block,
        out_shape=jax.ShapeDtypeStruct((n_ep, toks, width), BF16),
        name="mix",
    )(tok, wgt, dot, picked)
    mixed = lax.psum_scatter(mixed, "ep", scatter_dimension=0, tiled=False).astype(F32)
    square = lax.psum(jnp.sum(mixed * mixed, axis=1), "tp")
    scale = lax.rsqrt(square / (width * n_tp) + 1e-06)
    return (mixed * scale[:, None] * gain[None, :]).astype(BF16)


def solution(mesh):
    placed = (P("ep", "tp"), P("ep", None), P("ep", None), P("ep", "tp"), P("ep", "tp"), P("tp"))
    return jax.shard_map(body, mesh=mesh, in_specs=placed, out_specs=P("ep", "tp"), check_vma=False)
```

time: 282 us -> 535 us (1.90); the launches traced: 281 us -> 527 us
  waiting for transfers between devices: 49.6 us -> 315 us
  local copies, waits for them, and re-layouts: 131 us -> 0.67 us
  Pallas kernels: 0 us -> 79.1 us
  blocking collectives: 36.4 us -> 111 us
  starting transfers between devices: 48.8 us -> 4.64 us
  between operations: 0.26 us -> 13.4 us
  other arithmetic: 13.2 us -> 3.37 us
    unnamed x0 -> x3, waiting for transfers between devices: none -> 253 us
    gather x4 -> x0, local copies, waits for them, and re-layouts: 97.3 us -> none  [the longest x1 29.2 us: body(): contrib = (act[:, :, None] * out_table[ids]).astype(jnp.bfloat16)]
    pallas_call x0 -> x3, Pallas kernels: none -> 79.1 us  [the longest x1 40.9 us: body(): pl.pallas_call(dots_kernel, grid_spec=pltpu.PrefetchScalarGridSpec(num_sc...]
    psum x0 -> x2, blocking collectives: none -> 76.1 us  [the longest x1 47.6 us: body(): dot = lax.psum(dot, 'tp')]
    all_gather x0 -> x1, waiting for transfers between devices: none -> 51.9 us  [body(): feat = lax.all_gather(tokens, 'ep')]
    all_to_all x3 -> x1, starting transfers between devices: 48.8 us -> 4.59 us  [body(): ids = exchange(ids)]
    all_to_all x3 -> x1, waiting for transfers between devices: 49.6 us -> 10.1 us  [body(): ids = exchange(ids)]
    scatter x2 -> x0, local copies, waits for them, and re-layouts: 31.6 us -> none  [the longest x1 16.1 us: body(): jnp.zeros((n_ep * capacity,), jnp.int32).at[position].set(local_row)]
  transfers between devices with their start and end apart: 3 -> 3, of which waited for: 1 -> 3; matrix products, arithmetic and copies ran while one was open for 37% -> 0% of each run, Pallas kernels for 0% -> 1%
where the time goes in v1:
time: 535 us; the launch traced here: 527 us
  waiting for transfers between devices  315 us (59%)
  blocking collectives  111 us (21%)
  Pallas kernels  79.1 us (15%)
  between operations  13.4 us (3%)
    unnamed x3, waiting for transfers between devices  253 us
    all_gather x1, waiting for transfers between devices, body(): feat = lax.all_gather(tokens, 'ep')  51.9 us
    psum x1, blocking collectives, body(): dot = lax.psum(dot, 'tp')  47.6 us
    pallas_call x1, Pallas kernels, body(): pl.pallas_call(dots_kernel, grid_spec=pltpu.PrefetchScalarGridSpec(num_sc...  40.9 us
    all_to_all x1, blocking collectives, body(): tokwgt = exchange(jnp.stack([tok, wgt], axis=1))  34.8 us
    pallas_call x1, Pallas kernels, body(): pl.pallas_call(mix_kernel, grid=(n_ep,), in_specs=[lane, lane, lane, rows...  34.7 us
    psum x1, blocking collectives, body(): square = lax.psum(jnp.sum(mixed * mixed, axis=1), 'tp')  28.4 us
  transfers between devices with their start and end apart: 3, of which 3 were waited for; matrix products, arithmetic and copies ran while one was open for 0% of the time, Pallas kernels for 1%

profile of v1, /device:TPU:1, one launch (start us, length us, event | category | flops | bytes accessed | tf_op | source)
XLA Modules:
  0.0 527.4 jit_solution(7349596228959589737)
XLA Ops:
  6.5 0.0 all-gather.3.cloned.1.call-start
  6.5 0.7 all-gather.3.cloned.1.call-update
  7.3 3.5 bucket.1
  10.8 0.8 pad_maximum_fusion
  11.6 34.8 %all_to_all.16 = f32[64,2,128]{2,1,0:T(2,128)S(1)} all-to-all(f32[64,2,128]{2,1,0:T(2,128)S(1)} %pad_maximum_fusion), channel_id=1, replica_groups=mesh['ep'=64,'tp'=16] {'ep'}, dimensions={0} | all-to-all | bytes 131072 | tf_op jit(solution)/shard_map/all_to_all | solution.py:104
  46.5 4.6 all-to-all-start.1
  51.1 0.0 reduce-scatter.4.cloned.1.call-start
  51.1 0.7 fusion.3
  51.8 10.1 %all-to-all-done.1 = s32[64,1,128]{2,1,0:T(1,128)S(1)} async-done(((s32[64,1,128]{2,1,0:T(1,128)}), s32[64,1,128]{2,1,0:T(1,128)S(1)}, u32[]{:S(2)}, u32[]{:S(2)}) %all-to-all-start.1) | async-done | bytes 32800 | tf_op jit(solution)/shard_map/all_to_all | solution.py:103
  61.8 0.0 copy-start
  61.8 51.9 %all-gather.3.cloned.1.call-done = bf16[16384,128]{1,0:T(8,128)(2,1)} async-done(((bf16[256,128]{1,0:T(8,128)(2,1)}), bf16[16384,128]{1,0:T(8,128)(2,1)}) %all-gather.3.cloned.1.call-update) | async-done | bytes 4194320 | tf_op jit(solution)/shard_map/all_gather | solution.py:105
  113.7 0.0 copy-done
  113.7 40.9 %dots.1 = (f32[64,1,128]{2,1,0:T(1,128)}, bf16[64,128,128]{2,1,0:T(8,128)(2,1)}) custom-call(s32[64,128]{1,0:T(8,128)} %bitcast.15, f32[64,1,128]{2,1,0:T(1,128)} %get-tuple-element.16.tok_ref, bf16[64,256,128]{2,1,0:T(8,128)(2,1)} %bitcast.14, bf16[4096,128]{1,0:T(8,128)(2,1)} %up_ref.1, bf16[4096,128]{1,0:T(8,128)(2,1)} %out_ref.1), custom_call_target="tpu_custom_call" | custom-call | tf_op jit(solution)/shard_map/dots/pallas_call | solution.py:111
  154.5 47.6 %psum.14.dot_ref = f32[64,1,128]{2,1,0:T(1,128)} all-reduce(f32[64,1,128]{2,1,0:T(1,128)} %get-tuple-element.13), channel_id=1, replica_groups=mesh['ep'=64,'tp'=16] {'tp'}, use_global_device_ids=true, to_apply=%region_0.0 | all-reduce | flops 8192 | bytes 65536 | tf_op jit(solution)/shard_map/psum | solution.py:126
  202.2 0.0 copy-start.1
  202.2 34.7 %mix.1 = bf16[64,256,128]{2,1,0:T(8,128)(2,1)} custom-call(f32[64,1,128]{2,1,0:T(1,128)} %get-tuple-element.16.tok_ref, f32[64,1,128]{2,1,0:T(1,128)} %get-tuple-element.15.wgt_ref, f32[64,1,128]{2,1,0:T(1,128)} %psum.14.dot_ref, bf16[64,128,128]{2,1,0:T(8,128)(2,1)} %get-tuple-element.14.rows_ref), custom_call_target="tpu_custom_call" | custom-call | tf_op jit(solution)/shard_map/mix/pallas_call | solution.py:127
  236.9 0.0 reduce-scatter.4.cloned.1.call-update
  236.9 252.7 %reduce-scatter.4.cloned.1.call-done = bf16[1,256,128]{2,1,0:T(8,128)(2,1)} async-done(((bf16[64,256,128]{2,1,0:T(8,128)(2,1)}), bf16[1,256,128]{2,1,0:T(8,128)(2,1)}) %reduce-scatter.4.cloned.1.call-update) | async-done | bytes 65552
  489.6 0.9 fusion
  490.6 28.4 %psum.15 = f32[256]{0:T(256)S(1)} all-reduce(f32[256]{0:T(256)S(1)} %fusion), channel_id=1, replica_groups=mesh['ep'=64,'tp'=16] {'tp'}, use_global_device_ids=true, to_apply=%region_3.0 | all-reduce | flops 256 | bytes 2048 | tf_op jit(solution)/shard_map/psum | solution.py:136
  519.0 0.0 copy-done.1
  519.0 1.6 fusion.2
  (1 shorter events, 0.0 us)
Async XLA Ops:
  6.5 107.2 %all-gather.3.cloned.1.call-start = ((), (), s32[]{:S(2)}) async-start(), calls=%async_computation.3 | async-start | bytes 4259840 | tf_op jit(solution)/shard_map/all_gather | solution.py:105
  46.5 15.4 %all-to-all-start.1 = ((s32[64,1,128]{2,1,0:T(1,128)}), s32[64,1,128]{2,1,0:T(1,128)S(1)}, u32[]{:S(2)}, u32[]{:S(2)}) async-start(s32[64,1,128]{2,1,0:T(1,128)} %bitcast.16), calls=%async_computation.1 | async-start | bytes 65536 | tf_op jit(solution)/shard_map/all_to_all | solution.py:103
  51.1 438.6 %reduce-scatter.4.cloned.1.call-start = ((), (), s32[]{:S(2)}) async-start(), calls=%async_computation.4 | async-start | bytes 4259840
  61.8 51.9 %copy-start = (s32[64,1,128]{2,1,0:T(1,128)}, s32[64,1,128]{2,1,0:T(1,128)S(1)}, u32[]{:S(2)}) copy-start(s32[64,1,128]{2,1,0:T(1,128)S(1)} %all-to-all-done.1) | copy-start | bytes 98308
  202.2 316.8 %copy-start.1 = (f32[128]{0:T(128)S(1)}, f32[128]{0:T(128)}, u32[]{:S(2)}) copy-start(f32[128]{0:T(128)} %param.11) | copy-start | bytes 1540
Sparse Core Ops, SparseCore 0:
  11.6 102.0 all-gather.2
  237.1 252.5 reduce-scatter.3

commit v2 on v1

--- a/solution.py
+++ b/solution.py
@@ -9,6 +9,101 @@
 
 F32, BF16, I32 = jnp.float32, jnp.bfloat16, jnp.int32
 CONTRACT_MINOR = (((1,), (1,)), ((), ()))
+MESH = pl.DeviceIdType.MESH
+ANY = pl.BlockSpec(memory_space=pl.ANY)
+VMEM = pl.BlockSpec(memory_space=pltpu.VMEM)
+
+
+def distance(ring, step):
+    return min(step, ring - step)
+
+
+def heading(ring, step, plus):
+    if step == 0:
+        return 0
+    if 2 * step == ring:
+        return 1 if plus else -1
+    return 1 if 2 * step < ring else -1
+
+
+def beyond(ring, step, plus):
+    out = []
+    for way in (1, -1):
+        after = (step + way) % ring
+        if after and step in (0, after - way, (after - way) % ring):
+            if heading(ring, after, plus) == way and (step == 0 or heading(ring, step, plus) == way):
+                out.append(way)
+    return out
+
+
+def wave(ring):
+    every = [(q, p) for q in range(ring) for p in range(ring)]
+    far = lambda qp: (distance(ring, qp[0]) + distance(ring, qp[1]), distance(ring, qp[1]), qp)
+    return sorted(every, key=far)
+
+
+def neighbours(ring):
+    me = lax.axis_index("ep")
+    z, y = me // ring, lax.rem(me, ring)
+    up = lambda k: lax.rem(k + 1, ring)
+    down = lambda k: lax.rem(k + ring - 1, ring)
+    return z, y, {
+        (0, 1): up(z) * ring + y,
+        (0, -1): down(z) * ring + y,
+        (1, 1): z * ring + up(y),
+        (1, -1): z * ring + down(y),
+    }
+
+
+def greet(near):
+    barrier = pltpu.get_barrier_semaphore()
+    for device in near.values():
+        pl.semaphore_signal(barrier, inc=1, device_id={"ep": device}, device_id_type=MESH)
+    pl.semaphore_wait(barrier, len(near))
+
+
+def arrived(ref, sem):
+    pltpu.make_async_copy(ref, ref, sem).wait()
+
+
+def gather_kernel(ring, x_ref, all_ref, send_sem, recv_sem, load_sem):
+    _, _, near = neighbours(ring)
+    rows = all_ref.shape[3]
+    loads = [
+        pltpu.make_async_copy(x_ref.at[pl.ds(h * rows, rows)], all_ref.at[h, 0, 0], load_sem.at[h])
+        for h in range(2)
+    ]
+    for load in loads:
+        load.start()
+    greet(near)
+    for load in loads:
+        load.wait()
+    sent = []
+
+    def send(h, q, p, axis, way):
+        after = ((q + way) % ring, p) if axis == h else (q, (p + way) % ring)
+        copy = pltpu.make_async_remote_copy(
+            all_ref.at[h, q, p],
+            all_ref.at[h, *after],
+            send_sem.at[len(sent)],
+            recv_sem.at[h, *after],
+            device_id={"ep": near[axis, way]},
+            device_id_type=MESH,
+        )
+        copy.start()
+        sent.append(copy)
+
+    for q, p in wave(ring):
+        for h in range(2):
+            if (q, p) != (0, 0):
+                arrived(all_ref.at[h, q, p], recv_sem.at[h, q, p])
+            if p == 0:
+                for way in beyond(ring, q, h == 0):
+                    send(h, q, p, h, way)
+            for way in beyond(ring, p, q % 2 == 0):
+                send(h, q, p, 1 - h, way)
+    for copy in sent:
+        copy.wait_send()
 
 
 def bucket_kernel(rows_held, expert_ref, weight_ref, id_ref, tok_ref, wgt_ref):
@@ -50,11 +145,11 @@
     wgt_ref[...] = part[3] + part[4]
 
 
-def dots_kernel(id_ref, tok_ref, feat_ref, up_ref, out_ref, dot_ref, rows_ref, table, pair):
+def dots_kernel(id_ref, tok_ref, feat_a, feat_b, up_ref, out_ref, dot_ref, rows_ref, table, pair):
     step = pl.program_id(0)
     held = up_ref.shape[0]
     cap = id_ref.shape[1]
-    toks = feat_ref.shape[1]
+    half = feat_a.shape[3]
 
     @pl.when(step == 0)
     def _():
@@ -66,31 +161,101 @@
         pair[2 * r : 2 * r + 2, :] = table[pl.ds(pl.multiple_of(row * 2, 2), 2), :]
     up = pair[pl.ds(0, cap, stride=2), :].astype(BF16)
     rows_ref[0] = pair[pl.ds(1, cap, stride=2), :].astype(BF16)
-    every = lax.dot_general(feat_ref[0], up, CONTRACT_MINOR, preferred_element_type=F32)
+    token = lax.broadcasted_iota(I32, (half, cap), 0).astype(F32)
+    total = jnp.zeros((1, cap), F32)
+    for h, feat in enumerate((feat_a, feat_b)):
+        every = lax.dot_general(feat[0, 0, 0], up, CONTRACT_MINOR, preferred_element_type=F32)
+        here = tok_ref[0] - float(h * half) == token
+        total = total + jnp.sum(jnp.where(here, every, 0.0), axis=0, keepdims=True)
+    dot_ref[0] = total
+
+
+def reduce_kernel(ring, tok_ref, coef_ref, rows_ref, mixed_ref, part, inbox, extra, inbox2, outbox, send_sem, recv_sem):
+    z, y, near = neighbours(ring)
+    toks = part.shape[1]
+    rows = toks // 2
+    cap = tok_ref.shape[2]
+    greet(near)
     token = lax.broadcasted_iota(I32, (toks, cap), 0).astype(F32)
-    dot_ref[0] = jnp.sum(jnp.where(tok_ref[0] == token, every, 0.0), axis=0, keepdims=True)
-
-
-def mix_kernel(tok_ref, wgt_ref, dot_ref, rows_ref, mixed_ref):
-    toks = mixed_ref.shape[1]
-    cap = tok_ref.shape[2]
-    coef = jax.nn.gelu(dot_ref[0]) * wgt_ref[0]
-    coef_hi = coef.astype(BF16).astype(F32)
-    token = lax.broadcasted_iota(I32, (toks, cap), 0).astype(F32)
-    here = tok_ref[0] == token
-    spread = jnp.concatenate(
-        [jnp.where(here, c, 0.0).astype(BF16) for c in (coef_hi, coef - coef_hi)], axis=1
-    )
-    rows = jnp.concatenate([rows_ref[0]] * 2, axis=0)
-    mixed_ref[0] = jnp.dot(spread, rows, preferred_element_type=F32).astype(mixed_ref.dtype)
+
+    def one(s, carry):
+        q, p = s // ring, lax.rem(s, ring)
+        source = lax.rem(z + ring - q, ring) * ring + lax.rem(y + ring - p, ring)
+        here = tok_ref[source] == token
+        coef = coef_ref[source]
+        coef_hi = coef.astype(BF16).astype(F32)
+        spread = jnp.concatenate(
+            [jnp.where(here, c, 0.0).astype(BF16) for c in (coef_hi, coef - coef_hi)], axis=1
+        )
+        picked = rows_ref[source]
+        both = jnp.concatenate([picked, picked], axis=0)
+        part[s] = jnp.dot(spread, both, preferred_element_type=F32)
+        return carry
+
+    lax.fori_loop(0, ring * ring, one, 0)
+    sent = []
+
+    def send(h, q, p, value, target, slot, axis, way):
+        outbox[h, q, p] = value.astype(BF16)
+        copy = pltpu.make_async_remote_copy(
+            outbox.at[h, q, p],
+            target,
+            send_sem.at[len(sent)],
+            recv_sem.at[slot],
+            device_id={"ep": near[axis, way]},
+            device_id_type=MESH,
+        )
+        copy.start()
+        sent.append(copy)
+
+    number = {}
+
+    def slot_of(*key):
+        return number.setdefault(key, len(number))
+
+    def box(h, q, p, way):
+        return (extra.at[h, q], slot_of("x", h, q)) if p == 0 and way < 0 else (inbox.at[h, q, p], slot_of("i", h, q, p))
+
+    def box2(h, q, way):
+        return (inbox2.at[h, ring], slot_of("x2", h)) if q == 0 and way < 0 else (inbox2.at[h, q], slot_of("i2", h, q))
+
+    for q, p in reversed(wave(ring)):
+        for h in range(2):
+            u, v = (q, p) if h == 0 else (p, q)
+            value = part[u * ring + v, h * rows : (h + 1) * rows]
+            plus = q % 2 == 0
+            for way in beyond(ring, p, plus):
+                ref, slot = box(h, q, p, way)
+                arrived(ref, recv_sem.at[slot])
+                value = value + ref[...].astype(F32)
+            if p:
+                way = heading(ring, p, plus)
+                ref, slot = box(h, q, (p - way) % ring, way)
+                send(h, q, p, value, ref, slot, 1 - h, -way)
+                continue
+            for way in beyond(ring, q, h == 0):
+                ref, slot = box2(h, q, way)
+                arrived(ref, recv_sem.at[slot])
+                value = value + ref[...].astype(F32)
+            if q:
+                way = heading(ring, q, h == 0)
+                ref, slot = box2(h, (q - way) % ring, way)
+                send(h, q, p, value, ref, slot, h, -way)
+                continue
+            mixed_ref[h * rows : (h + 1) * rows, :] = value
+    for copy in sent:
+        copy.wait_send()
 
 
 def body(tokens, experts, weights, up_table, out_table, gain):
     n_ep, n_tp = lax.axis_size("ep"), lax.axis_size("tp")
+    ring = round(n_ep**0.5)
     toks, width = tokens.shape
     slots = experts.shape[1]
     held = up_table.shape[0]
     cap = 2 * toks * slots // n_ep
+    half = toks // 2
+    z, y, _ = neighbours(ring)
     listed = jax.ShapeDtypeStruct((n_ep, cap), F32)
     ids, tok, wgt = pl.pallas_call(
         functools.partial(bucket_kernel, held),
@@ -102,18 +267,36 @@
     )
     ids = exchange(ids)
     tokwgt = exchange(jnp.stack([tok, wgt], axis=1))
-    feat = lax.all_gather(tokens, "ep")
+    feat = pl.pallas_call(
+        functools.partial(gather_kernel, ring),
+        out_shape=jax.ShapeDtypeStruct((2, ring, ring, half, width), BF16),
+        in_specs=[ANY],
+        out_specs=VMEM,
+        scratch_shapes=[
+            pltpu.SemaphoreType.DMA((2 * (n_ep - 1),)),
+            pltpu.SemaphoreType.DMA((2, ring, ring)),
+            pltpu.SemaphoreType.DMA((2,)),
+        ],
+        compiler_params=pltpu.CompilerParams(collective_id=0, has_side_effects=True),
+        name="gather",
+    )(tokens)
     tok, wgt = tokwgt[:, :1], tokwgt[:, 1:]
+
+    def turn(s, me_z, me_y):
+        return lax.rem(me_z + ring - s // ring, ring) , lax.rem(me_y + ring - lax.rem(s, ring), ring)
+
+    place = jnp.stack([z, y]).astype(I32)
     lane = pl.BlockSpec((1, 1, cap), lambda s, *_: (s, 0, 0))
     whole = pl.BlockSpec((held, width), lambda s, *_: (0, 0))
-    block = pl.BlockSpec((1, toks, width), lambda s, *_: (s, 0, 0))
+    feat_a = pl.BlockSpec((1, 1, 1, half, width), lambda s, ids, pos: (0, *turn(s, pos[0], pos[1]), 0, 0))
+    feat_b = pl.BlockSpec((1, 1, 1, half, width), lambda s, ids, pos: (1, *turn(s, pos[0], pos[1])[::-1], 0, 0))
     rows = pl.BlockSpec((1, cap, width), lambda s, *_: (s, 0, 0))
     dot, picked = pl.pallas_call(
-        dots_kernel,
+        lambda ids, pos, *refs: dots_kernel(ids, *refs),
         grid_spec=pltpu.PrefetchScalarGridSpec(
-            num_scalar_prefetch=1,
+            num_scalar_prefetch=2,
             grid=(n_ep,),
-            in_specs=[lane, block, whole, whole],
+            in_specs=[lane, feat_a, feat_b, whole, whole],
             out_specs=[lane, rows],
             scratch_shapes=[pltpu.VMEM((2 * held, width), F32), pltpu.VMEM((2 * cap, width), F32)],
         ),
@@ -122,17 +305,27 @@
             jax.ShapeDtypeStruct((n_ep, cap, width), BF16),
         ),
         name="dots",
-    )(ids, tok, feat, up_table, out_table)
+    )(ids, place, tok, feat, feat, up_table, out_table)
     dot = lax.psum(dot, "tp")
+    coef = jax.nn.gelu(dot) * wgt
+    messages = 2 * (n_ep - 1)
     mixed = pl.pallas_call(
-        mix_kernel,
-        grid=(n_ep,),
-        in_specs=[lane, lane, lane, rows],
-        out_specs=block,
-        out_shape=jax.ShapeDtypeStruct((n_ep, toks, width), BF16),
-        name="mix",
-    )(tok, wgt, dot, picked)
-    mixed = lax.psum_scatter(mixed, "ep", scatter_dimension=0, tiled=False).astype(F32)
+        functools.partial(reduce_kernel, ring),
+        out_shape=jax.ShapeDtypeStruct((toks, width), F32),
+        in_specs=[VMEM] * 3,
+        out_specs=VMEM,
+        scratch_shapes=[
+            pltpu.VMEM((n_ep, toks, width), F32),
+            pltpu.VMEM((2, ring, ring, half, width), BF16),
+            pltpu.VMEM((2, ring, half, width), BF16),
+            pltpu.VMEM((2, ring + 1, half, width), BF16),
+            pltpu.VMEM((2, ring, ring, half, width), BF16),
+            pltpu.SemaphoreType.DMA((messages,)),
+            pltpu.SemaphoreType.DMA((messages,)),
+        ],
+        compiler_params=pltpu.CompilerParams(collective_id=1, has_side_effects=True),
+        name="reduce",
+    )(tok, coef, picked)
     square = lax.psum(jnp.sum(mixed * mixed, axis=1), "tp")
     scale = lax.rsqrt(square / (width * n_tp) + 1e-06)
     return (mixed * scale[:, None] * gain[None, :]).astype(BF16)

time: 535 us -> 256 us (0.48)
  waiting for transfers between devices: 315 us -> 9.67 us
  Pallas kernels: 79.1 us -> 123 us
  blocking collectives: 111 us -> 79.7 us
  starting transfers between devices: 4.64 us -> 32.5 us
  between operations: 13.4 us -> 0.08 us
    unnamed x3 -> x0, waiting for transfers between devices: 253 us -> none
    all_gather x1 -> x0, waiting for transfers between devices: 51.9 us -> none  [body(): feat = lax.all_gather(tokens, 'ep')]
    pallas_call x2 -> x3, Pallas kernels: 75.6 us -> 119 us  [the longest x1 42.6 us: body(): pl.pallas_call(functools.partial(reduce_kernel, ring), out_shape=jax.Shap...]
    all_to_all x1 -> x0, blocking collectives: 34.8 us -> none  [body(): tokwgt = exchange(jnp.stack([tok, wgt], axis=1))]
    all_to_all x0 -> x1, starting transfers between devices: none -> 23.9 us  [body(): tokwgt = exchange(jnp.stack([tok, wgt], axis=1))]
  transfers between devices with their start and end apart: 3 -> 2, of which waited for: 3 -> 1; matrix products, arithmetic and copies ran while one was open for 0% -> 0% of each run, Pallas kernels for 1% -> 15%
where the time goes in v2:
time: 256 us; the launch traced here: 251 us
  Pallas kernels  123 us (48%)
  blocking collectives  79.7 us (31%)
  starting transfers between devices  32.5 us (13%)
  waiting for transfers between devices  9.67 us (4%)
  other arithmetic  5.42 us (2%)
    psum x1, blocking collectives, body(): dot = lax.psum(dot, 'tp')  49.6 us
    pallas_call x1, Pallas kernels, body(): pl.pallas_call(functools.partial(reduce_kernel, ring), out_shape=jax.Shap...  42.6 us
    pallas_call x1, Pallas kernels, body(): pl.pallas_call(lambda ids, pos, *refs: dots_kernel(ids, *refs), grid_spec...  39.4 us
    pallas_call x1, Pallas kernels, body(): pl.pallas_call(functools.partial(gather_kernel, ring), out_shape=jax.Shap...  36.9 us
    psum x1, blocking collectives, body(): square = lax.psum(jnp.sum(mixed * mixed, axis=1), 'tp')  30.1 us
    all_to_all x1, starting transfers between devices, body(): tokwgt = exchange(jnp.stack([tok, wgt], axis=1))  23.9 us
    all_to_all x1, waiting for transfers between devices, body(): ids = exchange(ids)  9.67 us
    all_to_all x1, starting transfers between devices, body(): ids = exchange(ids)  8.54 us
  transfers between devices with their start and end apart: 2, of which 1 were waited for; matrix products, arithmetic and copies ran while one was open for 0% of the time, Pallas kernels for 15%

profile of v2, /device:TPU:1, one launch (start us, length us, event | category | flops | bytes accessed | tf_op | source)
XLA Modules:
  0.0 251.1 jit_solution(17894811217005113886)
XLA Ops:
  0.0 3.5 %bucket.1 = (s32[64,128]{1,0:T(8,128)}, f32[64,128]{1,0:T(8,128)}, f32[64,128]{1,0:T(8,128)}) custom-call(s32[16,256]{1,0:T(8,128)} %bitcast.13, f32[16,256]{1,0:T(8,128)} %bitcast.14), custom_call_target="tpu_custom_call" | custom-call | tf_op jit(solution)/shard_map/bucket/pallas_call | solution.py:260
  3.5 1.5 pad_maximum_fusion
  5.0 23.9 %all-to-all-start = ((f32[64,2,128]{2,1,0:T(2,128)}), f32[64,2,128]{2,1,0:T(2,128)S(1)}, u32[]{:S(2)}, u32[]{:S(2)}) async-start(f32[64,2,128]{2,1,0:T(2,128)} %pad_maximum_fusion), calls=%async_computation | async-start | bytes 131072 | tf_op jit(solution)/shard_map/all_to_all | solution.py:269
  29.0 36.9 %gather.1.refs_1_.refs_2_ = bf16[2,8,8,128,128]{4,3,2,1,0:T(8,128)(2,1)} custom-call(bf16[256,128]{1,0:T(8,128)(2,1)} %x_ref.1), custom_call_target="tpu_custom_call" | custom-call | tf_op jit(solution)/shard_map/gather/pallas_call | solution.py:270
  65.9 0.0 all-to-all-done
  65.9 8.5 %all-to-all-start.1 = ((s32[64,1,128]{2,1,0:T(1,128)}), s32[64,1,128]{2,1,0:T(1,128)S(1)}, u32[]{:S(2)}, u32[]{:S(2)}) async-start(s32[64,1,128]{2,1,0:T(1,128)} %bitcast.5), calls=%async_computation.1 | async-start | bytes 65536 | tf_op jit(solution)/shard_map/all_to_all | solution.py:268
  74.5 0.6 pad_add_fusion.pos
  75.1 0.6 slice.8.refs_0_.tok_ref
  75.7 9.7 %all-to-all-done.1 = s32[64,1,128]{2,1,0:T(1,128)S(1)} async-done(((s32[64,1,128]{2,1,0:T(1,128)}), s32[64,1,128]{2,1,0:T(1,128)S(1)}, u32[]{:S(2)}, u32[]{:S(2)}) %all-to-all-start.1) | async-done | bytes 32800 | tf_op jit(solution)/shard_map/all_to_all | solution.py:268
  85.4 0.0 copy-start
  85.4 0.6 copy-done
  86.0 0.0 copy-start.1
  86.0 39.4 %dots.1 = (f32[64,1,128]{2,1,0:T(1,128)}, bf16[64,128,128]{2,1,0:T(8,128)(2,1)}) custom-call(s32[64,128]{1,0:T(8,128)} %bitcast.10, s32[2]{0:T(128)} %pad_add_fusion.pos, f32[64,1,128]{2,1,0:T(1,128)} %slice.8.refs_0_.tok_ref, bf16[2,8,8,128,128]{4,3,2,1,0:T(8,128)(2,1)} %gather.1.refs_1_.refs_2_, bf16[2,8,8,128,128]{4,3,2,1,0:T(8,128)(2,1)} %gather.1.refs_1_.refs_2_, ...), custom_call_target="tpu_custom_call" | custom-call | tf_op jit(solution)/shard_map/dots/pallas_call | solution.py:294
  125.4 49.6 %psum.14 = f32[64,1,128]{2,1,0:T(1,128)S(1)} all-reduce(f32[64,1,128]{2,1,0:T(1,128)} %get-tuple-element.13), channel_id=1, replica_groups=mesh['ep'=64,'tp'=16] {'tp'}, use_global_device_ids=true, to_apply=%region_0.1 | all-reduce | flops 8192 | bytes 65536 | tf_op jit(solution)/shard_map/psum | solution.py:309
  175.0 0.7 fusion.7.coef_ref
  175.7 42.6 %reduce.1 = f32[256,128]{1,0:T(8,128)} custom-call(f32[64,1,128]{2,1,0:T(1,128)} %slice.8.refs_0_.tok_ref, f32[64,1,128]{2,1,0:T(1,128)} %fusion.7.coef_ref, bf16[64,128,128]{2,1,0:T(8,128)(2,1)} %get-tuple-element.14.rows_ref), custom_call_target="tpu_custom_call" | custom-call | tf_op jit(solution)/shard_map/reduce/pallas_call | solution.py:312
  218.4 1.0 multiply_reduce_fusion
  219.4 30.1 %psum.15 = f32[256]{0:T(256)S(1)} all-reduce(f32[256]{0:T(256)S(1)} %multiply_reduce_fusion), channel_id=1, replica_groups=mesh['ep'=64,'tp'=16] {'tp'}, use_global_device_ids=true, to_apply=%region_2.3 | all-reduce | flops 256 | bytes 2048 | tf_op jit(solution)/shard_map/psum | solution.py:329
  249.5 0.0 copy-done.1
  249.5 1.6 multiply_convert_fusion
  (1 shorter events, 0.0 us)
Async XLA Ops:
  5.0 60.9 %all-to-all-start = ((f32[64,2,128]{2,1,0:T(2,128)}), f32[64,2,128]{2,1,0:T(2,128)S(1)}, u32[]{:S(2)}, u32[]{:S(2)}) async-start(f32[64,2,128]{2,1,0:T(2,128)} %pad_maximum_fusion), calls=%async_computation | async-start | bytes 131072 | tf_op jit(solution)/shard_map/all_to_all | solution.py:269
  65.9 19.4 %all-to-all-start.1 = ((s32[64,1,128]{2,1,0:T(1,128)}), s32[64,1,128]{2,1,0:T(1,128)S(1)}, u32[]{:S(2)}, u32[]{:S(2)}) async-start(s32[64,1,128]{2,1,0:T(1,128)} %bitcast.5), calls=%async_computation.1 | async-start | bytes 65536 | tf_op jit(solution)/shard_map/all_to_all | solution.py:268
  85.4 0.6 copy-start
  86.0 163.5 %copy-start.1 = (f32[128]{0:T(128)S(1)}, f32[128]{0:T(128)}, u32[]{:S(2)}) copy-start(f32[128]{0:T(128)} %param.11) | copy-start | bytes 1540

commit v3 on v1

v3 whole, which is shorter than its diff:
```python
import functools

import jax
import jax.numpy as jnp
from jax import lax
from jax.experimental import pallas as pl
from jax.experimental.pallas import tpu as pltpu
from jax.sharding import PartitionSpec as P

F32, BF16, I32 = jnp.float32, jnp.bfloat16, jnp.int32
CONTRACT_MINOR = (((1,), (1,)), ((), ()))
MESH = pl.DeviceIdType.MESH
BATCHES = 4
GATHERS = 4
MIXES = 8


def distance(ring, step):
    return min(step, ring - step)


def heading(ring, step, plus):
    if step == 0:
        return 0
    if 2 * step == ring:
        return 1 if plus else -1
    return 1 if 2 * step < ring else -1


def beyond(ring, step, plus):
    out = []
    for way in (1, -1):
        after = (step + way) % ring
        if after and heading(ring, after, plus) == way and (step == 0 or heading(ring, step, plus) == way):
            out.append(way)
    return out


def wave(ring):
    every = [(u, v) for u in range(ring) for v in range(ring)]
    return sorted(every, key=lambda uv: (-distance(ring, uv[0]) - distance(ring, uv[1]), uv))


def arrived(ref, sem):
    pltpu.make_async_copy(ref, ref, sem).wait()


def bucket_kernel(rows_held, expert_ref, weight_ref, code_ref, share_ref):
    slots, toks = expert_ref.shape
    ring, _, cap = code_ref.shape
    owners = ring * ring
    shift = rows_held.bit_length() - 1
    owner_no = lax.broadcasted_iota(I32, (owners, toks), 0)
    rank_no = lax.broadcasted_iota(I32, (cap, toks), 0)
    token_no = lax.broadcasted_iota(I32, (1, toks), 1).astype(F32)
    first = lax.broadcasted_iota(I32, (toks, toks), 0)
    second = lax.broadcasted_iota(I32, (toks, toks), 1)
    earlier = jnp.where(first < second, 1.0, 0.0).astype(BF16)
    ones = jnp.ones((toks, toks), BF16)
    before = jnp.zeros((owners, toks), F32)
    found = jnp.zeros((5 * owners, cap), F32)
    for k in range(slots):
        expert = expert_ref[k : k + 1, :]
        local = expert & (rows_held - 1)
        mine = (expert >> shift) == owner_no
        onehot = jnp.where(mine, 1.0, 0.0).astype(BF16)
        rank = before + jnp.dot(onehot, earlier, preferred_element_type=F32)
        before = before + jnp.dot(onehot, ones, preferred_element_type=F32)
        rank = jnp.sum(jnp.where(mine, rank, 0.0), axis=0, keepdims=True).astype(I32)
        place = jnp.where(rank == rank_no, 1.0, 0.0).astype(BF16)
        weight = weight_ref[k : k + 1, :]
        weight_hi = weight.astype(BF16).astype(F32)
        pieces = (
            (local >> 8).astype(F32),
            (local & 255).astype(F32),
            token_no,
            weight_hi,
            weight - weight_hi,
        )
        what = jnp.concatenate([jnp.where(mine, p, 0.0).astype(BF16) for p in pieces], axis=0)
        found = found + lax.dot_general(what, place, CONTRACT_MINOR, preferred_element_type=F32)
    part = [found[i * owners : (i + 1) * owners] for i in range(5)]
    code = part[2] * float(rows_held) + part[0] * 256.0 + part[1]
    weight = part[3] + part[4]
    for k in range(ring):
        code_ref[k] = code[k * ring : (k + 1) * ring].astype(I32)
        share_ref[k] = weight[k * ring : (k + 1) * ring]


def kernel(
    ring,
    n_tp,
    token_ref,
    code_ref,
    share_ref,
    up_ref,
    out_ref,
    gain_ref,
    normed_ref,
    feats,
    staged,
    table,
    pair,
    code_middle,
    code_onward,
    code_packs,
    share_middle,
    share_onward,
    share_packs,
    codes,
    shares,
    tokens,
    row_vmem,
    row_smem,
    ups,
    outs,
    dots,
    dot_box,
    coefs,
    parts,
    inbox,
    inbox_x,
    inbox2,
    outbox,
    squares,
    load_sem,
    feat_sem,
    middle_sem,
    pack_sem,
    row_sem,
    dot_sem,
    sum_sem,
    square_sem,
    sent_sem,
):
    blocks = ring * ring
    held = up_ref.shape[0]
    half = feats.shape[1]
    toks = 2 * half
    cap = codes.shape[1]
    order = wave(ring)
    number = {uv: i for i, uv in enumerate(order)}
    me, mine = lax.axis_index("ep"), lax.axis_index("tp")
    z, y = me // ring, lax.rem(me, ring)
    turn = lambda k, by: lax.rem(k + by % ring, ring)
    column = lambda by: {"ep": turn(z, by) * ring + y}
    line = lambda by: {"ep": z * ring + turn(y, by)}
    across = lambda by: {"tp": lax.rem(mine + by, n_tp)}
    along = (column, line)

    def remote(src, dst, sent, landed, device):
        pltpu.make_async_remote_copy(
            src, dst, sent, landed, device_id=device, device_id_type=MESH
        ).start()

    own = number[0, 0]
    loads = [
        pltpu.make_async_copy(token_ref.at[pl.ds(h * half, half)], feats.at[h * blocks + own], load_sem.at[h])
        for h in range(2)
    ]
    tables = [
        pltpu.make_async_copy(ref, staged.at[i], load_sem.at[2 + i])
        for i, ref in enumerate((up_ref, out_ref))
    ]
    for load in loads + tables:
        load.start()
    barrier = pltpu.get_barrier_semaphore()
    peers = [f(by) for f in along for by in range(1, ring)] + [across(by) for by in range(1, n_tp)]
    for peer in peers:
        pl.semaphore_signal(barrier, inc=1, device_id=peer, device_id_type=MESH)
    for load in loads:
        load.wait()
    pl.semaphore_wait(barrier, len(peers))

    def place(h, q, p):
        return h * blocks + number[(q, p) if h == 0 else (p, q)]

    def pass_on(h, q, p):
        here = place(h, q, p)
        if (q, p) != (0, 0):
            arrived(feats.at[here], feat_sem.at[here])
        hops = [(h, way, place(h, (q + way) % ring, 0)) for way in beyond(ring, q, h == 0) if p == 0]
        hops += [(1 - h, way, place(h, q, (p + way) % ring)) for way in beyond(ring, p, q % 2 == 0)]
        for axis, way, there in hops:
            remote(feats.at[here], feats.at[there], sent_sem.at[0], feat_sem.at[there], along[axis](way))

    gathering = [functools.partial(pass_on, h, q, p) for q, p in reversed(order) for h in range(2)]

    parcels = (
        (code_ref, code_middle, code_onward, code_packs, codes),
        (share_ref, share_middle, share_onward, share_packs, shares),
    )

    def send_parcels():
        for kind, (parcel, middle, _, _, _) in enumerate(parcels):
            for by in range(1, ring):
                remote(parcel.at[turn(z, by)], middle.at[by], sent_sem.at[1 + kind], middle_sem.at[kind, by], column(by))
            middle[0] = parcel[z]

    def build_table():
        for load in tables:
            load.wait()
        for i in range(2):
            table[pl.ds(i, held, stride=2), :] = staged[i].astype(F32)

    def forward_parcels():
        for kind, (_, middle, onward, packs, _) in enumerate(parcels):
            for by in range(1, ring):
                arrived(middle.at[by], middle_sem.at[kind, by])
            for k in range(ring):
                for u in range(ring):
                    onward[k, u : u + 1, :] = middle[u, k : k + 1, :]
            for by in range(1, ring):
                remote(onward.at[turn(y, by)], packs.at[by], sent_sem.at[3 + kind], pack_sem.at[kind, by], line(by))
            packs[0] = onward[y]

    def open_packs():
        for kind, (_, _, _, packs, listed) in enumerate(parcels):
            for by in range(1, ring):
                arrived(packs.at[by], pack_sem.at[kind, by])
            for i, (u, v) in enumerate(order):
                listed[i : i + 1, :] = packs[v, u : u + 1, :]
        code = codes[...]
        row_vmem[...] = (code & (held - 1)) * 2
        tokens[...] = (code >> (held.bit_length() - 1)).astype(F32)

    def fetch_rows():
        copy = pltpu.make_async_copy(row_vmem, row_smem, row_sem)
        copy.start()
        copy.wait()

    def gather(start):
        def one(i, carry):
            for r in range(cap):
                pair[2 * r : 2 * r + 2, :] = table[pl.ds(row_smem[i, r], 2), :]
            ups[i] = pair[pl.ds(0, cap, stride=2), :].astype(BF16)
            outs[i] = pair[pl.ds(1, cap, stride=2), :].astype(BF16)
            return carry

        lax.fori_loop(start, start + GATHERS, one, 0)

    def interleave(first, second):
        done = 0
        for k, step in enumerate(first):
            step()
            upto = (k + 1) * len(second) // len(first)
            for step in second[done:upto]:
                step()
            done = upto

    early, middle_part, late = gathering[:2], gathering[2:34], gathering[34:]
    for step in early:
        step()
    send_parcels()
    for step in middle_part[:24]:
        step()
    forward_parcels()
    build_table()
    for step in middle_part[24:]:
        step()
    open_packs()
    for step in late[:4]:
        step()
    fetch_rows()
    interleave(late[4:], [functools.partial(gather, s) for s in range(0, blocks, GATHERS)])

    batch = blocks // BATCHES
    token = lax.broadcasted_iota(I32, (toks, cap), 0).astype(F32)

    def take_dots(b):
        def one(i, carry):
            feat = jnp.concatenate([feats[i], feats[blocks + i]], axis=0)
            every = lax.dot_general(feat, ups[i], CONTRACT_MINOR, preferred_element_type=F32)
            here = tokens[pl.ds(i, 1), :] == token
            dots[pl.ds(i, 1), :] = jnp.sum(jnp.where(here, every, 0.0), axis=0, keepdims=True)
            return carry

        lax.fori_loop(b * batch, (b + 1) * batch, one, 0)
        for by in range(1, n_tp):
            remote(
                dots.at[pl.ds(b * batch, batch)], dot_box.at[b, by], sent_sem.at[5 + b], dot_sem.at[b], across(by)
            )

    def take_coefs(b):
        arrived(dot_box.at[b, pl.ds(1, n_tp - 1)], dot_sem.at[b])
        which = slice(b * batch, (b + 1) * batch)
        total = dots[which, :]
        for by in range(1, n_tp):
            total = total + dot_box[b, by]
        coefs[which, :] = jax.nn.gelu(total) * shares[which, :]

    def mix(start):
        def one(i, carry):
            here = tokens[pl.ds(i, 1), :] == token
            coef = coefs[pl.ds(i, 1), :]
            coef_hi = coef.astype(BF16).astype(F32)
            spread = jnp.concatenate(
                [jnp.where(here, c, 0.0).astype(BF16) for c in (coef_hi, coef - coef_hi)], axis=1
            )
            both = jnp.concatenate([outs[i]] * 2, axis=0)
            parts[i] = jnp.dot(spread, both, preferred_element_type=F32)
            return carry

        lax.fori_loop(start, start + MIXES, one, 0)

    slots = {}

    def sem_of(*key):
        return sum_sem.at[slots.setdefault(key, len(slots))]

    def box(h, q, p, way):
        if p == 0 and way < 0:
            return inbox_x.at[h, q], sem_of("x", h, q)
        return inbox.at[place(h, q, p)], sem_of("i", h, q, p)

    def box2(h, q, way):
        if q == 0 and way < 0:
            return inbox2.at[h, ring], sem_of("x2", h)
        return inbox2.at[h, q], sem_of("i2", h, q)

    mixed = [None, None]

    def add_up(h, q, p):
        here = place(h, q, p)
        value = parts[here - h * blocks, h * half : (h + 1) * half]
        plus = q % 2 == 0
        came = [box(h, q, p, way) for way in beyond(ring, p, plus)]
        if p == 0:
            came += [box2(h, q, way) for way in beyond(ring, q, h == 0)]
        for ref, sem in came:
            arrived(ref, sem)
            value = value + ref[...].astype(F32)
        if (q, p) == (0, 0):
            mixed[h] = value
            return
        outbox[here] = value.astype(BF16)
        if p:
            way = heading(ring, p, plus)
            (ref, sem), axis = box(h, q, (p - way) % ring, way), 1 - h
        else:
            way = heading(ring, q, h == 0)
            (ref, sem), axis = box2(h, (q - way) % ring, way), h
        remote(outbox.at[here], ref, sent_sem.at[5 + BATCHES], sem, along[axis](-way))

    for b in range(BATCHES):
        take_dots(b)
    for b in range(BATCHES):
        take_coefs(b)
        for s in range(b * batch, (b + 1) * batch, MIXES):
            mix(s)
            for i in range(s, s + MIXES):
                for h in range(2):
                    add_up(h, *order[i][:: 1 - 2 * h])

    ones = jnp.ones((8, 2 * normed_ref.shape[1]), BF16)
    sums = []
    for h in range(2):
        square = mixed[h] * mixed[h]
        square_hi = square.astype(BF16).astype(F32)
        split = jnp.concatenate([square_hi.astype(BF16), (square - square_hi).astype(BF16)], axis=1)
        sums.append(lax.dot_general(ones, split, CONTRACT_MINOR, preferred_element_type=F32))
    which = lax.broadcasted_iota(I32, sums[0].shape, 0)
    squares[0] = jnp.where(which == 0, sums[0], sums[1])[:2]
    for by in range(1, n_tp):
        remote(squares.at[0], squares.at[by], sent_sem.at[6 + BATCHES], square_sem, across(by))
    arrived(squares.at[pl.ds(1, n_tp - 1)], square_sem)
    total = squares[0]
    for by in range(1, n_tp):
        total = total + squares[by]
    scale = lax.rsqrt(total / (normed_ref.shape[1] * n_tp) + 1e-06)
    same = lax.broadcasted_iota(I32, (half, half), 0) == lax.broadcasted_iota(I32, (half, half), 1)
    for h in range(2):
        scales = jnp.sum(jnp.where(same, scale[h : h + 1, :], 0.0), axis=1, keepdims=True)
        normed_ref[h * half : (h + 1) * half, :] = (mixed[h] * scales * gain_ref[...]).astype(BF16)

    arrived(feats.at[pl.ds(0, 2 * (blocks - 1))], sent_sem.at[0])
    for kind, (_, middle, _, packs, _) in enumerate(parcels):
        arrived(middle.at[pl.ds(1, ring - 1)], sent_sem.at[1 + kind])
        arrived(packs.at[pl.ds(1, ring - 1)], sent_sem.at[3 + kind])
    for b in range(BATCHES):
        arrived(dot_box.at[b, pl.ds(1, n_tp - 1)], sent_sem.at[5 + b])
    arrived(outbox.at[pl.ds(0, 2 * (blocks - 1))], sent_sem.at[5 + BATCHES])
    arrived(squares.at[pl.ds(1, n_tp - 1)], sent_sem.at[6 + BATCHES])


def body(tokens, experts, weights, up_table, out_table, gain):
    n_ep, n_tp = lax.axis_size("ep"), lax.axis_size("tp")
    ring = round(n_ep**0.5)
    toks, width = tokens.shape
    slots = experts.shape[1]
    held = up_table.shape[0]
    cap = 2 * toks * slots // n_ep
    half = toks // 2
    batch = n_ep // BATCHES
    any_space, vmem = pl.BlockSpec(memory_space=pl.ANY), pl.BlockSpec(memory_space=pltpu.VMEM)
    dma = pltpu.SemaphoreType.DMA
    codes, shares = pl.pallas_call(
        functools.partial(bucket_kernel, held),
        out_shape=(
            jax.ShapeDtypeStruct((ring, ring, cap), I32),
            jax.ShapeDtypeStruct((ring, ring, cap), F32),
        ),
        name="bucket",
    )(experts.T, weights.T)
    return pl.pallas_call(
        functools.partial(kernel, ring, n_tp),
        out_shape=jax.ShapeDtypeStruct((toks, width), BF16),
        in_specs=[any_space, vmem, vmem, any_space, any_space, vmem],
        out_specs=vmem,
        scratch_shapes=[
            pltpu.VMEM((2 * n_ep, half, width), BF16),
            pltpu.VMEM((2, held, width), BF16),
            pltpu.VMEM((2 * held, width), F32),
            pltpu.VMEM((2 * cap, width), F32),
            pltpu.VMEM((ring, ring, cap), I32),
            pltpu.VMEM((ring, ring, cap), I32),
            pltpu.VMEM((ring, ring, cap), I32),
            pltpu.VMEM((ring, ring, cap), F32),
            pltpu.VMEM((ring, ring, cap), F32),
            pltpu.VMEM((ring, ring, cap), F32),
            pltpu.VMEM((n_ep, cap), I32),
            pltpu.VMEM((n_ep, cap), F32),
            pltpu.VMEM((n_ep, cap), F32),
            pltpu.VMEM((n_ep, cap), I32),
            pltpu.SMEM((n_ep, cap), I32),
            pltpu.VMEM((n_ep, cap, width), BF16),
            pltpu.VMEM((n_ep, cap, width), BF16),
            pltpu.VMEM((n_ep, cap), F32),
            pltpu.VMEM((BATCHES, n_tp, batch, cap), F32),
            pltpu.VMEM((n_ep, cap), F32),
            pltpu.VMEM((n_ep, toks, width), F32),
            pltpu.VMEM((2 * n_ep, half, width), BF16),
            pltpu.VMEM((2, ring, half, width), BF16),
            pltpu.VMEM((2, ring + 1, half, width), BF16),
            pltpu.VMEM((2 * n_ep, half, width), BF16),
            pltpu.VMEM((n_tp, 2, half), F32),
            dma((4,)),
            dma((2 * n_ep,)),
            dma((2, ring)),
            dma((2, ring)),
            dma,
            dma((BATCHES,)),
            dma((2 * n_ep,)),
            dma,
            dma((7 + BATCHES,)),
        ],
        compiler_params=pltpu.CompilerParams(
            collective_id=0, has_side_effects=True, vmem_limit_bytes=56 << 20
        ),
        name="retrieve",
    )(tokens, codes, shares, up_table, out_table, gain[None, :])


def solution(mesh):
    placed = (P("ep", "tp"), P("ep", None), P("ep", None), P("ep", "tp"), P("ep", "tp"), P("tp"))
    return jax.shard_map(body, mesh=mesh, in_specs=placed, out_specs=P("ep", "tp"), check_vma=False)
```

time: 535 us -> 132 us (0.25); the launches traced: 527 us -> 132 us
  waiting for transfers between devices: 315 us -> 0 us
  blocking collectives: 111 us -> 0 us
  Pallas kernels: 79.1 us -> 130 us
  between operations: 13.4 us -> 0.01 us
    unnamed x3 -> x0, waiting for transfers between devices: 253 us -> none
    psum x2 -> x0, blocking collectives: 76.1 us -> none  [the longest x1 47.6 us: body(): dot = lax.psum(dot, 'tp')]
    all_gather x1 -> x0, waiting for transfers between devices: 51.9 us -> none  [body(): feat = lax.all_gather(tokens, 'ep')]
    pallas_call x2 -> x1, Pallas kernels: 75.6 us -> 127 us  [body(): pl.pallas_call(functools.partial(kernel, ring, n_tp), out_shape=jax.Shape...]
    all_to_all x1 -> x0, blocking collectives: 34.8 us -> none  [body(): tokwgt = exchange(jnp.stack([tok, wgt], axis=1))]
    all_to_all x1 -> x0, waiting for transfers between devices: 10.1 us -> none  [body(): ids = exchange(ids)]
  transfers between devices with their start and end apart: 3 -> 0, of which waited for: 3 -> 0; matrix products, arithmetic and copies ran while one was open for 0% -> 0% of each run, Pallas kernels for 1% -> 0%
where the time goes in v3:
time: 132 us
  Pallas kernels  130 us (98%)
  local copies, waits for them, and re-layouts  1.47 us (1%)
    pallas_call x1, Pallas kernels, body(): pl.pallas_call(functools.partial(kernel, ring, n_tp), out_shape=jax.Shape...  127 us
    pallas_call x1, Pallas kernels, body(): pl.pallas_call(functools.partial(bucket_kernel, held), out_shape=(jax.Sha...  3.53 us

profile of v3, /device:TPU:1, one launch (start us, length us, event | category | flops | bytes accessed | tf_op | source)
XLA Modules:
  0.0 131.7 jit_solution(11326189683630352901)
XLA Ops:
  0.0 3.5 %bucket.1 = (s32[8,8,128]{2,1,0:T(8,128)}, f32[8,8,128]{2,1,0:T(8,128)}) custom-call(s32[16,256]{1,0:T(8,128)} %bitcast.3, f32[16,256]{1,0:T(8,128)} %bitcast.4), custom_call_target="tpu_custom_call" | custom-call | tf_op jit(solution)/shard_map/bucket/pallas_call | solution.py:397
  3.5 126.6 %retrieve.1 = bf16[256,128]{1,0:T(8,128)(2,1)} custom-call(bf16[256,128]{1,0:T(8,128)(2,1)} %token_ref.1, s32[8,8,128]{2,1,0:T(8,128)} %get-tuple-element.7.code_ref, f32[8,8,128]{2,1,0:T(8,128)} %get-tuple-element.8.share_ref, bf16[4096,128]{1,0:T(8,128)(2,1)} %up_ref.1, bf16[4096,128]{1,0:T(8,128)(2,1)} %out_ref.1, f32[1,128]{1,0:T(1,128)} %bitcast.5), custom_call_target="tpu_custom_call" | custom-call | tf_op jit(solution)/shard_map/retrieve/pallas_call | solution.py:405
  130.2 1.5 %copy.8 = bf16[256,128]{1,0:T(8,128)(2,1)} copy(bf16[256,128]{1,0:T(8,128)(2,1)} %retrieve.1) | data formatting | bytes 131072

commit v4 on v3

v4 whole, which is shorter than its diff:
```python
import functools

import jax
import jax.numpy as jnp
from jax import lax
from jax.experimental import pallas as pl
from jax.experimental.pallas import tpu as pltpu
from jax.sharding import PartitionSpec as P

F32, BF16, I32 = jnp.float32, jnp.bfloat16, jnp.int32
CONTRACT_MINOR = (((1,), (1,)), ((), ()))
MESH = pl.DeviceIdType.MESH
scope = jax.named_scope
CHUNKS = 2
BATCHES = 8
GATHERS = 2
UNROLL = 4
SLACK = 0.6
LATER = 10.0


def distance(ring, step):
    return min(step, ring - step)


def heading(ring, step, plus):
    if step == 0:
        return 0
    if 2 * step == ring:
        return 1 if plus else -1
    return 1 if 2 * step < ring else -1


def beyond(ring, step, plus):
    out = []
    for way in (1, -1):
        after = (step + way) % ring
        if after and heading(ring, after, plus) == way and (step == 0 or heading(ring, step, plus) == way):
            out.append(way)
    return out


def wave(ring):
    every = [(u, v) for u in range(ring) for v in range(ring)]
    return sorted(every, key=lambda uv: (-distance(ring, uv[0]) - distance(ring, uv[1]), uv))


def schedule(steps, slack, late):
    users = {}
    for name, (_, needs, _) in steps.items():
        for need in needs:
            users.setdefault(need, []).append(name)
    rank = {}
    pending = [(name, False) for name in steps]
    while pending:
        name, ready = pending.pop()
        ways = [(user, 0.0) for user in users.get(name, [])]
        ways += [(user, t + under_way) for _, t, under_way, m in steps[name][2] for user in users.get(m, [])]
        if ready:
            rank[name] = steps[name][0] + max((wait + rank[user] for user, wait in ways), default=0.0)
        elif name not in rank:
            pending.append((name, True))
            pending += [(user, False) for user, _ in ways if user not in rank]
    waits = {name: len(needs) for name, (_, needs, _) in steps.items()}
    at = {name: 0.0 for name in steps}
    ready = [name for name in steps if not waits[name]]
    now, busy, order = 0.0, {}, []

    def tell(key, time):
        for user in users.get(key, []):
            at[user] = max(at[user], time)
            waits[user] -= 1
            if not waits[user]:
                ready.append(user)

    def start(name):
        return max([at[name]] + [busy.get(link, 0.0) - slack for link, _, _, _ in steps[name][2] if link])

    while ready:
        starts = {name: start(name) for name in ready}
        now = max(now, min(starts.values()))
        name = max((n for n in ready if starts[n] <= now + 1e-9), key=lambda n: rank[n] - late(n))
        ready.remove(name)
        order.append(name)
        now += steps[name][0]
        tell(name, now)
        for link, t, under_way, m in steps[name][2]:
            begin = max(now, busy.get(link, 0.0)) if link else now
            busy[link] = begin + t
            tell(m, begin + t + under_way)
    assert len(order) == len(steps)
    return order


def arrived(ref, sem):
    pltpu.make_async_copy(ref, ref, sem).wait()


def bucket_kernel(
    rows_held, expert_hbm, weight_hbm, token_hbm, code_ref, share_ref, token_ref, expert_ref, weight_ref, load_sem
):
    loads = [
        pltpu.make_async_copy(src, dst, load_sem.at[i])
        for i, (src, dst) in enumerate(((expert_hbm, expert_ref), (weight_hbm, weight_ref), (token_hbm, token_ref)))
    ]
    for load in loads:
        load.start()
    slots, toks = expert_ref.shape
    ring, _, cap = code_ref.shape
    owners = ring * ring
    shift = rows_held.bit_length() - 1
    owner_no = lax.broadcasted_iota(I32, (owners, toks), 0)
    rank_no = lax.broadcasted_iota(I32, (cap, toks), 0)
    token_no = lax.broadcasted_iota(I32, (1, toks), 1).astype(F32)
    first = lax.broadcasted_iota(I32, (toks, toks), 0)
    second = lax.broadcasted_iota(I32, (toks, toks), 1)
    earlier = jnp.where(first < second, 1.0, 0.0).astype(BF16)
    ones = jnp.ones((toks, toks), BF16)
    before = jnp.zeros((owners, toks), F32)
    found = jnp.zeros((5 * owners, cap), F32)
    for load in loads:
        load.wait()
    for k in range(slots):
        expert = expert_ref[k : k + 1, :]
        local = expert & (rows_held - 1)
        mine = (expert >> shift) == owner_no
        onehot = jnp.where(mine, 1.0, 0.0).astype(BF16)
        rank = before + jnp.dot(onehot, earlier, preferred_element_type=F32)
        before = before + jnp.dot(onehot, ones, preferred_element_type=F32)
        rank = jnp.sum(jnp.where(mine, rank, 0.0), axis=0, keepdims=True).astype(I32)
        place = jnp.where(rank == rank_no, 1.0, 0.0).astype(BF16)
        weight = weight_ref[k : k + 1, :]
        weight_hi = weight.astype(BF16).astype(F32)
        pieces = (
            (local >> 8).astype(F32),
            (local & 255).astype(F32),
            token_no,
            weight_hi,
            weight - weight_hi,
        )
        what = jnp.concatenate([jnp.where(mine, p, 0.0).astype(BF16) for p in pieces], axis=0)
        found = found + lax.dot_general(what, place, CONTRACT_MINOR, preferred_element_type=F32)
    part = [found[i * owners : (i + 1) * owners] for i in range(5)]
    code = part[2] * float(rows_held) + part[0] * 256.0 + part[1]
    weight = part[3] + part[4]
    for k in range(ring):
        code_ref[k] = code[k * ring : (k + 1) * ring].astype(I32)
        share_ref[k] = weight[k * ring : (k + 1) * ring]


def kernel(ring, *refs):
    messages = 2 * CHUNKS * ring * ring
    dma = pltpu.SemaphoreType.DMA
    pl.run_scoped(
        functools.partial(inside, ring, *refs),
        load_sem=dma((3,)),
        feat_sem=dma((messages,)),
        middle_sem=dma((2, ring)),
        pack_sem=dma((2, ring)),
        row_sem=dma,
        dot_sem=dma((CHUNKS * BATCHES,)),
        sum_sem=dma((messages,)),
        square_sem=dma((CHUNKS,)),
        sent_sem=dma((8,)),
    )


def inside(
    ring,
    n_tp,
    token_ref,
    code_ref,
    share_ref,
    up_ref,
    out_ref,
    gain_hbm,
    normed_ref,
    feats,
    gain_ref,
    staged,
    table,
    pair,
    code_middle,
    code_onward,
    code_packs,
    share_middle,
    share_onward,
    share_packs,
    codes,
    shares,
    tokens,
    row_vmem,
    row_smem,
    ups,
    outs,
    dots,
    dot_box,
    coefs,
    parts,
    inbox,
    inbox_x,
    inbox2,
    outbox,
    mixed,
    squares,
    *,
    load_sem,
    feat_sem,
    middle_sem,
    pack_sem,
    row_sem,
    dot_sem,
    sum_sem,
    square_sem,
    sent_sem,
):
    blocks = ring * ring
    held, width = up_ref.shape
    rows = feats.shape[1]
    span = 2 * rows
    cap = codes.shape[1]
    order = wave(ring)
    number = {uv: i for i, uv in enumerate(order)}
    me, mine = lax.axis_index("ep"), lax.axis_index("tp")
    z, y = me // ring, lax.rem(me, ring)
    turn = lambda k, by: lax.rem(k + by % ring, ring)
    column = lambda by: {"ep": turn(z, by) * ring + y}
    line = lambda by: {"ep": z * ring + turn(y, by)}
    across = lambda by: {"tp": lax.rem(mine + by, n_tp)}
    along = (column, line)
    place = lambda h, q, p: number[(q, p) if h == 0 else (p, q)]
    slot = lambda c, h, q, p: (c * 2 + h) * blocks + place(h, q, p)

    def remote(src, dst, sent, landed, device):
        pltpu.make_async_remote_copy(
            src, dst, sent, landed, device_id=device, device_id_type=MESH
        ).start()

    loads = [
        pltpu.make_async_copy(src, dst, load_sem.at[i])
        for i, (src, dst) in enumerate(
            ((up_ref, staged.at[0]), (out_ref, staged.at[1]), (gain_hbm, gain_ref))
        )
    ]
    for load in loads:
        load.start()
    barrier = pltpu.get_barrier_semaphore()
    peers = [f(by) for f in along for by in range(1, ring)] + [across(by) for by in range(1, n_tp)]
    for peer in peers:
        pl.semaphore_signal(barrier, inc=1, device_id=peer, device_id_type=MESH)

    steps, actions = {}, {}

    def step(name, time, needs, sends, action):
        steps[name] = (time, needs, sends)
        actions[name] = action

    wire = rows * width * 2 / 46.6e3
    hop = 2.0

    def pass_on(c, h, q, p):
        here = slot(c, h, q, p)
        hops = [(h, way, slot(c, h, (q + way) % ring, 0)) for way in beyond(ring, q, h == 0) if p == 0]
        hops += [(1 - h, way, slot(c, h, q, (p + way) % ring)) for way in beyond(ring, p, q % 2 == 0)]

        def action():
            if (q, p) == (0, 0):
                source = token_ref.at[pl.ds((c * 2 + h) * rows, rows)]
                feats[here] = source[...]
            else:
                source = feats.at[here]
                arrived(source, feat_sem.at[here])
            for axis, way, there in hops:
                remote(source, feats.at[there], sent_sem.at[0], feat_sem.at[there], along[axis](way))

        needs = [] if (q, p) == (0, 0) else [("feat", here)]
        sends = [((axis, way), wire, hop, ("feat", there)) for axis, way, there in hops]
        step(("pass", c, h, q, p), 0.02 + 0.01 * len(hops), needs, sends, action)

    for c in range(CHUNKS):
        for h in range(2):
            for q, p in order:
                pass_on(c, h, q, p)

    parcels = (
        (code_ref, code_middle, code_onward, code_packs, codes),
        (share_ref, share_middle, share_onward, share_packs, shares),
    )

    def send_parcels():
        for kind, (parcel, middle, _, _, _) in enumerate(parcels):
            for by in range(1, ring):
                remote(parcel.at[turn(z, by)], middle.at[by], sent_sem.at[1 + kind], middle_sem.at[kind, by], column(by))
            middle[0] = parcel[z]

    def forward_parcels():
        for kind, (_, middle, onward, packs, _) in enumerate(parcels):
            for by in range(1, ring):
                arrived(middle.at[by], middle_sem.at[kind, by])
            for k in range(ring):
                for u in range(ring):
                    onward[k, u : u + 1, :] = middle[u, k : k + 1, :]
            for by in range(1, ring):
                remote(onward.at[turn(y, by)], packs.at[by], sent_sem.at[3 + kind], pack_sem.at[kind, by], line(by))
            packs[0] = onward[y]

    def open_packs():
        for kind, (_, _, _, packs, listed) in enumerate(parcels):
            for by in range(1, ring):
                arrived(packs.at[by], pack_sem.at[kind, by])
            for i, (u, v) in enumerate(order):
                listed[i : i + 1, :] = packs[v, u : u + 1, :]
        code = codes[...]
        row_vmem[...] = (code & (held - 1)) * 2
        tokens[...] = (code >> (held.bit_length() - 1)).astype(F32)

    fetch = pltpu.make_async_copy(row_vmem, row_smem, row_sem)
    letters = lambda axis, what: [((axis, way), 0.7, 4.0, (what, way)) for way in (1, -1)]
    step("send_parcels", 0.05, [], letters(0, "middle"), send_parcels)
    step("forward_parcels", 0.1, [("middle", 1), ("middle", -1)], letters(1, "pack"), forward_parcels)
    step("open_packs", 0.08, [("pack", 1), ("pack", -1)], [(None, 0.0, 0.1, "listed")], open_packs)
    step("fetch_rows", 0.02, ["listed"], [(None, 0.0, 1.1, "fetched")], fetch.start)
    step("rows", 0.01, ["fetched"], [], fetch.wait)

    def build_table():
        for load in loads:
            load.wait()
        for i in range(2):
            table[pl.ds(i, held, stride=2), :] = staged[i].astype(F32)

    step("build_table", 0.3, [], [], build_table)

    def gather(start):
        def one(i, carry):
            for r in range(cap):
                pair[2 * r : 2 * r + 2, :] = table[pl.ds(row_smem[i, r], 2), :]
            ups[i] = pair[pl.ds(0, cap, stride=2), :].astype(BF16)
            outs[i] = pair[pl.ds(1, cap, stride=2), :].astype(BF16)
            return carry

        lax.fori_loop(start, start + GATHERS, one, 0)

    for i in range(0, blocks, GATHERS):
        step(("gather", i), 0.125 * GATHERS, ["rows", "build_table"], [], functools.partial(gather, i))

    batch = blocks // BATCHES
    sublane = lax.broadcasted_iota(I32, (8, cap), 0).astype(F32)
    token = lax.broadcasted_iota(I32, (span, cap), 0).astype(F32)

    def in_fours(b, one):
        def four(k, carry):
            for i in range(UNROLL):
                one(b * batch + k * UNROLL + i)
            return carry

        lax.fori_loop(0, batch // UNROLL, four, 0)

    def take_dots(c, b):
        def one(i):
            feat = jnp.concatenate([feats[(c * 2 + h) * blocks + i] for h in range(2)], axis=0)
            every = lax.dot_general(feat, ups[i], CONTRACT_MINOR, preferred_element_type=F32)
            here = tokens[pl.ds(i, 1), :] - (sublane + float(c * span))
            sums = [None] * 4
            for g in range(span // 8):
                term = jnp.where(here == float(8 * g), every[8 * g : 8 * g + 8, :], 0.0)
                sums[g % 4] = term if sums[g % 4] is None else sums[g % 4] + term
            total = (sums[0] + sums[1]) + (sums[2] + sums[3])
            dots[c, pl.ds(i, 1), :] = jnp.sum(total, axis=0, keepdims=True)

        in_fours(b, one)
        some = pl.ds(b * batch, batch)
        for by in range(1, n_tp):
            remote(
                dots.at[c, some], dot_box.at[c, by, some], sent_sem.at[5], dot_sem.at[c * BATCHES + b], across(by)
            )

    def take_coefs(c, b):
        low, high = b * batch, (b + 1) * batch
        arrived(dot_box.at[c, pl.ds(1, n_tp - 1), pl.ds(low, batch)], dot_sem.at[c * BATCHES + b])
        total = dots[c, low:high, :]
        for by in range(1, n_tp):
            total = total + dot_box[c, by, low:high]
        coefs[c, low:high, :] = jax.nn.gelu(total) * shares[low:high, :]

        def one(i):
            here = tokens[pl.ds(i, 1), :] - float(c * span) == token
            coef = coefs[c, pl.ds(i, 1), :]
            coef_hi = coef.astype(BF16).astype(F32)
            spread = jnp.concatenate(
                [jnp.where(here, x, 0.0).astype(BF16) for x in (coef_hi, coef - coef_hi)], axis=1
            )
            both = jnp.concatenate([outs[i]] * 2, axis=0)
            parts[c, i] = jnp.dot(spread, both, preferred_element_type=F32)

        in_fours(b, one)

    share = 1.5 / CHUNKS
    for c in range(CHUNKS):
        for b in range(BATCHES):
            mine_of = range(b * batch, (b + 1) * batch)
            needs = [("gather", i) for i in mine_of if i % GATHERS == 0]
            needs += [("pass", c, h, *order[i][:: 1 - 2 * h]) for i in mine_of for h in range(2)]
            sends = [(("x",), 0.175 * batch, 5.0, ("totals", c, b))]
            step(("dots", c, b), 0.1 + 0.055 * batch * share, needs, sends, functools.partial(take_dots, c, b))
            step(("mix", c, b), 0.05 + 0.055 * batch * share, [("totals", c, b)], [], functools.partial(take_coefs, c, b))

    numbers = {}

    def box(*key):
        sem = sum_sem.at[numbers.setdefault(key, len(numbers))]
        kind, c, h, q, p, way = key
        if kind == 1:
            if p == 0 and way < 0:
                return inbox_x.at[(c * 2 + h) * ring + q], sem
            return inbox.at[slot(c, h, q, p)], sem
        return inbox2.at[(c * 2 + h) * (ring + 1) + (ring if q == 0 and way < 0 else q)], sem

    def add_up(c, h, q, p):
        here = slot(c, h, q, p)
        plus = q % 2 == 0
        came = [(1, c, h, q, p, way if p == 0 else 0) for way in beyond(ring, p, plus)]
        if p == 0:
            came += [(2, c, h, q, 0, way if q == 0 else 0) for way in beyond(ring, q, h == 0)]
        if p:
            way, axis = heading(ring, p, plus), 1 - h
            after = (p - way) % ring
            target = (1, c, h, q, after, way if after == 0 else 0)
        elif q:
            way, axis = heading(ring, q, h == 0), h
            after = (q - way) % ring
            target = (2, c, h, after, 0, way if after == 0 else 0)
        else:
            target = None

        def action():
            value = parts[c, place(h, q, p), h * rows : (h + 1) * rows]
            for key in came:
                ref, sem = box(*key)
                arrived(ref, sem)
                value = value + ref[...].astype(F32)
            if target is None:
                mixed[c, h * rows : (h + 1) * rows] = value
                return
            outbox[here] = value.astype(BF16)
            ref, sem = box(*target)
            remote(outbox.at[here], ref, sent_sem.at[6], sem, along[axis](-way))

        needs = [("mix", c, place(h, q, p) // batch)] + [("sum", *key) for key in came]
        sends = [((axis, -way), wire, hop, ("sum", *target))] if target else []
        step(("add", c, h, q, p), 0.02 + 0.03 / CHUNKS, needs, sends, action)

    for c in range(CHUNKS):
        for h in range(2):
            for q, p in order:
                add_up(c, h, q, p)

    def send_squares(c):
        square = mixed[c] * mixed[c]
        square_hi = square.astype(BF16).astype(F32)
        split = jnp.concatenate([square_hi.astype(BF16), (square - square_hi).astype(BF16)], axis=1)
        ones = jnp.ones((8, 2 * width), BF16)
        sums = lax.dot_general(ones, split, CONTRACT_MINOR, preferred_element_type=F32)
        squares[c, 0] = sums[:1]
        for by in range(1, n_tp):
            remote(squares.at[c, 0], squares.at[c, by], sent_sem.at[7], square_sem.at[c], across(by))

    def finish(c):
        arrived(squares.at[c, pl.ds(1, n_tp - 1)], square_sem.at[c])
        total = squares[c, 0]
        for by in range(1, n_tp):
            total = total + squares[c, by]
        scale = lax.rsqrt(total / (width * n_tp) + 1e-06)
        same = lax.broadcasted_iota(I32, (span, span), 0) == lax.broadcasted_iota(I32, (span, span), 1)
        scales = jnp.sum(jnp.where(same, scale, 0.0), axis=1, keepdims=True)
        normed_ref[c * span : (c + 1) * span, :] = (mixed[c] * scales * gain_ref[...]).astype(BF16)

    for c in range(CHUNKS):
        needs = [("add", c, h, 0, 0) for h in range(2)]
        step(("square", c), 0.2, needs, [(("x",), 0.4, 5.0, ("squares", c))], functools.partial(send_squares, c))
        step(("norm", c), 0.3, [("squares", c)], [], functools.partial(finish, c))

    chunk_of = lambda name: name[1] if isinstance(name, tuple) and name[0] != "gather" else 0
    plan = schedule(steps, SLACK, lambda name: LATER * chunk_of(name))
    with scope("barrier"):
        pl.semaphore_wait(barrier, len(peers))
    for name in plan:
        with scope(name if isinstance(name, str) else "_".join(map(str, name))):
            actions[name]()

    with scope("drain"):
        sums = CHUNKS * 2 * (blocks - 1)
        arrived(feats.at[pl.ds(0, sums)], sent_sem.at[0])
        for kind, (_, middle, _, packs, _) in enumerate(parcels):
            arrived(middle.at[pl.ds(1, ring - 1)], sent_sem.at[1 + kind])
            arrived(packs.at[pl.ds(1, ring - 1)], sent_sem.at[3 + kind])
        arrived(dot_box.at[:, pl.ds(1, n_tp - 1)], sent_sem.at[5])
        arrived(outbox.at[pl.ds(0, sums)], sent_sem.at[6])
        arrived(squares.at[:, pl.ds(1, n_tp - 1)], sent_sem.at[7])


def body(tokens, experts, weights, up_table, out_table, gain):
    n_ep, n_tp = lax.axis_size("ep"), lax.axis_size("tp")
    ring = round(n_ep**0.5)
    toks, width = tokens.shape
    slots = experts.shape[1]
    held = up_table.shape[0]
    cap = 2 * toks * slots // n_ep
    rows = toks // (2 * CHUNKS)
    blocks = 2 * CHUNKS * n_ep
    hbm, vmem = pl.BlockSpec(memory_space=pltpu.HBM), pl.BlockSpec(memory_space=pltpu.VMEM)
    in_hbm = lambda x: pltpu.with_memory_space_constraint(x, pltpu.HBM)
    codes, shares, near_tokens = pl.pallas_call(
        functools.partial(bucket_kernel, held),
        out_shape=(
            jax.ShapeDtypeStruct((ring, ring, cap), I32),
            jax.ShapeDtypeStruct((ring, ring, cap), F32),
            jax.ShapeDtypeStruct((toks, width), BF16),
        ),
        in_specs=[hbm] * 3,
        out_specs=(vmem, vmem, vmem),
        scratch_shapes=[
            pltpu.VMEM((slots, toks), I32),
            pltpu.VMEM((slots, toks), F32),
            pltpu.SemaphoreType.DMA((3,)),
        ],
        compiler_params=pltpu.CompilerParams(vmem_limit_bytes=4 << 20),
        name="bucket",
    )(in_hbm(experts.T), in_hbm(weights.T), in_hbm(tokens))
    return pl.pallas_call(
        functools.partial(kernel, ring, n_tp),
        out_shape=jax.ShapeDtypeStruct((toks, width), BF16),
        in_specs=[vmem, vmem, vmem, hbm, hbm, hbm],
        out_specs=vmem,
        scratch_shapes=[
            pltpu.VMEM((blocks, rows, width), BF16),
            pltpu.VMEM((1, width), F32),
            pltpu.VMEM((2, held, width), BF16),
            pltpu.VMEM((2 * held, width), F32),
            pltpu.VMEM((2 * cap, width), F32),
            pltpu.VMEM((ring, ring, cap), I32),
            pltpu.VMEM((ring, ring, cap), I32),
            pltpu.VMEM((ring, ring, cap), I32),
            pltpu.VMEM((ring, ring, cap), F32),
            pltpu.VMEM((ring, ring, cap), F32),
            pltpu.VMEM((ring, ring, cap), F32),
            pltpu.VMEM((n_ep, cap), I32),
            pltpu.VMEM((n_ep, cap), F32),
            pltpu.VMEM((n_ep, cap), F32),
            pltpu.VMEM((n_ep, cap), I32),
            pltpu.SMEM((n_ep, cap), I32),
            pltpu.VMEM((n_ep, cap, width), BF16),
            pltpu.VMEM((n_ep, cap, width), BF16),
            pltpu.VMEM((CHUNKS, n_ep, cap), F32),
            pltpu.VMEM((CHUNKS, n_tp, n_ep, cap), F32),
            pltpu.VMEM((CHUNKS, n_ep, cap), F32),
            pltpu.VMEM((CHUNKS, n_ep, 2 * rows, width), F32),
            pltpu.VMEM((blocks, rows, width), BF16),
            pltpu.VMEM((2 * CHUNKS * ring, rows, width), BF16),
            pltpu.VMEM((2 * CHUNKS * (ring + 1), rows, width), BF16),
            pltpu.VMEM((blocks, rows, width), BF16),
            pltpu.VMEM((CHUNKS, 2 * rows, width), F32),
            pltpu.VMEM((CHUNKS, n_tp, 1, 2 * rows), F32),
        ],
        compiler_params=pltpu.CompilerParams(
            collective_id=0, has_side_effects=True, vmem_limit_bytes=44 << 20
        ),
        name="retrieve",
    )(near_tokens, codes, shares, in_hbm(up_table), in_hbm(out_table), in_hbm(gain[None, :]))


def solution(mesh):
    placed = (P("ep", "tp"), P("ep", None), P("ep", None), P("ep", "tp"), P("ep", "tp"), P("tp"))
    return jax.shard_map(body, mesh=mesh, in_specs=placed, out_specs=P("ep", "tp"), check_vma=False)
```

time: 132 us -> 105 us (0.80)
  Pallas kernels: 130 us -> 104 us
    pallas_call x1, Pallas kernels: 127 us -> 101 us  [body(): pl.pallas_call(functools.partial(kernel, ring, n_tp), out_shape=jax.Shape...]
where the time goes in v4:
time: 105 us
  Pallas kernels  104 us (99%)
    pallas_call x1, Pallas kernels, body(): pl.pallas_call(functools.partial(kernel, ring, n_tp), out_shape=jax.Shape...  101 us
    pallas_call x1, Pallas kernels, body(): pl.pallas_call(functools.partial(bucket_kernel, held), out_shape=(jax.Sha...  3.08 us

profile of v4, /device:TPU:1, one launch (start us, length us, event | category | flops | bytes accessed | tf_op | source)
XLA Modules:
  0.0 104.8 jit_solution(13267761341204705748)
XLA Ops:
  0.0 3.1 %bucket.1 = (s32[8,8,128]{2,1,0:T(8,128)S(1)}, f32[8,8,128]{2,1,0:T(8,128)S(1)}, bf16[256,128]{1,0:T(8,128)(2,1)S(1)}) custom-call(s32[16,256]{1,0:T(8,128)} %bitcast.3, f32[16,256]{1,0:T(8,128)} %bitcast.4, bf16[256,128]{1,0:T(8,128)(2,1)} %token_hbm.1), custom_call_target="tpu_custom_call" | custom-call | tf_op jit(solution)/shard_map/bucket/pallas_call | solution.py:512
  3.1 101.1 %retrieve.1 = bf16[256,128]{1,0:T(8,128)(2,1)S(1)} custom-call(bf16[256,128]{1,0:T(8,128)(2,1)S(1)} %get-tuple-element.8.refs_0_, s32[8,8,128]{2,1,0:T(8,128)S(1)} %get-tuple-element.9.refs_1_, f32[8,8,128]{2,1,0:T(8,128)S(1)} %get-tuple-element.10.refs_2_, bf16[4096,128]{1,0:T(8,128)(2,1)} %refs_3_.1, bf16[4096,128]{1,0:T(8,128)(2,1)} %refs_4_.1, ...), custom_call_target="tpu_custom_call" | custom-call | tf_op jit(solution)/shard_map/retrieve/pallas_call | solution.py:529
  104.1 0.6 copy.8

commit v5 on v4

--- a/solution.py
+++ b/solution.py
@@ -11,12 +11,16 @@
 CONTRACT_MINOR = (((1,), (1,)), ((), ()))
 MESH = pl.DeviceIdType.MESH
 scope = jax.named_scope
+HOP = {(0, 1): 2.2, (0, -1): 2.4, (1, 1): 2.4, (1, -1): 2.4}
+WIRE, SLACK, ACROSS, LETTER, PICK = 0.36, 0.4, 6, 5, 0.165
+SOONER = {
+    ("pass", 0): 11, ("pass", 1): 2, ("dots", 0): -12, ("dots", 1): -14, ("mix", 0): 19,
+    ("mix", 1): 2, ("add", 0): 14, ("add", 1): -5, ("gather", 0): 7,
+}
+NEXT_BATCH = 6
 CHUNKS = 2
 BATCHES = 8
 GATHERS = 2
-UNROLL = 4
-SLACK = 0.6
-LATER = 10.0
 
 
 def distance(ring, step):
@@ -38,6 +42,10 @@
         if after and heading(ring, after, plus) == way and (step == 0 or heading(ring, step, plus) == way):
             out.append(way)
     return out
+
+
+def far_first(ring):
+    return sorted(range(1, ring), key=lambda by: -distance(ring, by))
 
 
 def wave(ring):
@@ -115,20 +123,23 @@
     first = lax.broadcasted_iota(I32, (toks, toks), 0)
     second = lax.broadcasted_iota(I32, (toks, toks), 1)
     earlier = jnp.where(first < second, 1.0, 0.0).astype(BF16)
-    ones = jnp.ones((toks, toks), BF16)
-    before = jnp.zeros((owners, toks), F32)
-    found = jnp.zeros((5 * owners, cap), F32)
+    ones = jnp.ones((toks, 128), BF16)
     for load in loads:
         load.wait()
+    experts = [expert_ref[k : k + 1, :] for k in range(slots)]
+    mine = [(expert >> shift) == owner_no for expert in experts]
+    onehot = jnp.concatenate([jnp.where(m, 1.0, 0.0).astype(BF16) for m in mine], axis=0)
+    ahead = jnp.dot(onehot, earlier, preferred_element_type=F32)
+    total = jnp.dot(onehot, ones, preferred_element_type=F32)
+    before = jnp.zeros((owners, ones.shape[1]), F32)
+    what, where = [], []
     for k in range(slots):
-        expert = expert_ref[k : k + 1, :]
-        local = expert & (rows_held - 1)
-        mine = (expert >> shift) == owner_no
-        onehot = jnp.where(mine, 1.0, 0.0).astype(BF16)
-        rank = before + jnp.dot(onehot, earlier, preferred_element_type=F32)
-        before = before + jnp.dot(onehot, ones, preferred_element_type=F32)
-        rank = jnp.sum(jnp.where(mine, rank, 0.0), axis=0, keepdims=True).astype(I32)
-        place = jnp.where(rank == rank_no, 1.0, 0.0).astype(BF16)
+        rows = slice(k * owners, (k + 1) * owners)
+        rank = ahead[rows] + jnp.concatenate([before] * (toks // ones.shape[1]), axis=1)
+        before = before + total[rows]
+        rank = jnp.sum(jnp.where(mine[k], rank, 0.0), axis=0, keepdims=True).astype(I32)
+        where.append(jnp.where(rank == rank_no, 1.0, 0.0).astype(BF16))
+        local = experts[k] & (rows_held - 1)
         weight = weight_ref[k : k + 1, :]
         weight_hi = weight.astype(BF16).astype(F32)
         pieces = (
@@ -138,8 +149,10 @@
             weight_hi,
             weight - weight_hi,
         )
-        what = jnp.concatenate([jnp.where(mine, p, 0.0).astype(BF16) for p in pieces], axis=0)
-        found = found + lax.dot_general(what, place, CONTRACT_MINOR, preferred_element_type=F32)
+        what.append(jnp.concatenate([jnp.where(mine[k], p, 0.0).astype(BF16) for p in pieces], axis=0))
+    found = lax.dot_general(
+        jnp.concatenate(what, axis=1), jnp.concatenate(where, axis=1), CONTRACT_MINOR, preferred_element_type=F32
+    )
     part = [found[i * owners : (i + 1) * owners] for i in range(5)]
     code = part[2] * float(rows_held) + part[0] * 256.0 + part[1]
     weight = part[3] + part[4]
@@ -255,8 +268,7 @@
         steps[name] = (time, needs, sends)
         actions[name] = action
 
-    wire = rows * width * 2 / 46.6e3
-    hop = 2.0
+    wire = WIRE * 2 / CHUNKS
 
     def pass_on(c, h, q, p):
         here = slot(c, h, q, p)
@@ -274,8 +286,8 @@
                 remote(source, feats.at[there], sent_sem.at[0], feat_sem.at[there], along[axis](way))
 
         needs = [] if (q, p) == (0, 0) else [("feat", here)]
-        sends = [((axis, way), wire, hop, ("feat", there)) for axis, way, there in hops]
-        step(("pass", c, h, q, p), 0.02 + 0.01 * len(hops), needs, sends, action)
+        sends = [((axis, way), wire, HOP[axis, way], ("feat", there)) for axis, way, there in hops]
+        step(("pass", c, h, q, p), 0.02, needs, sends, action)
 
     for c in range(CHUNKS):
         for h in range(2):
@@ -289,7 +301,7 @@
 
     def send_parcels():
         for kind, (parcel, middle, _, _, _) in enumerate(parcels):
-            for by in range(1, ring):
+            for by in far_first(ring):
                 remote(parcel.at[turn(z, by)], middle.at[by], sent_sem.at[1 + kind], middle_sem.at[kind, by], column(by))
             middle[0] = parcel[z]
 
@@ -300,7 +312,7 @@
             for k in range(ring):
                 for u in range(ring):
                     onward[k, u : u + 1, :] = middle[u, k : k + 1, :]
-            for by in range(1, ring):
+            for by in far_first(ring):
                 remote(onward.at[turn(y, by)], packs.at[by], sent_sem.at[3 + kind], pack_sem.at[kind, by], line(by))
             packs[0] = onward[y]
 
@@ -315,7 +327,7 @@
         tokens[...] = (code >> (held.bit_length() - 1)).astype(F32)
 
     fetch = pltpu.make_async_copy(row_vmem, row_smem, row_sem)
-    letters = lambda axis, what: [((axis, way), 0.7, 4.0, (what, way)) for way in (1, -1)]
+    letters = lambda axis, what: [((axis, way), 0.7, LETTER, (what, way)) for way in (1, -1)]
     step("send_parcels", 0.05, [], letters(0, "middle"), send_parcels)
     step("forward_parcels", 0.1, [("middle", 1), ("middle", -1)], letters(1, "pack"), forward_parcels)
     step("open_packs", 0.08, [("pack", 1), ("pack", -1)], [(None, 0.0, 0.1, "listed")], open_packs)
@@ -331,45 +343,36 @@
     step("build_table", 0.3, [], [], build_table)
 
     def gather(start):
-        def one(i, carry):
+        for i in range(start, start + GATHERS):
+            both = pair.at[i % 2]
             for r in range(cap):
-                pair[2 * r : 2 * r + 2, :] = table[pl.ds(row_smem[i, r], 2), :]
-            ups[i] = pair[pl.ds(0, cap, stride=2), :].astype(BF16)
-            outs[i] = pair[pl.ds(1, cap, stride=2), :].astype(BF16)
-            return carry
-
-        lax.fori_loop(start, start + GATHERS, one, 0)
+                both[2 * r : 2 * r + 2, :] = table[pl.ds(row_smem[i, r], 2), :]
+            ups[i] = both[pl.ds(0, cap, stride=2), :].astype(BF16)
+            outs[i] = both[pl.ds(1, cap, stride=2), :].astype(BF16)
 
     for i in range(0, blocks, GATHERS):
-        step(("gather", i), 0.125 * GATHERS, ["rows", "build_table"], [], functools.partial(gather, i))
+        step(("gather", i), PICK, ["rows", "build_table"], [], functools.partial(gather, i))
 
     batch = blocks // BATCHES
     sublane = lax.broadcasted_iota(I32, (8, cap), 0).astype(F32)
     token = lax.broadcasted_iota(I32, (span, cap), 0).astype(F32)
-
-    def in_fours(b, one):
-        def four(k, carry):
-            for i in range(UNROLL):
-                one(b * batch + k * UNROLL + i)
-            return carry
-
-        lax.fori_loop(0, batch // UNROLL, four, 0)
 
     def take_dots(c, b):
         def one(i):
             feat = jnp.concatenate([feats[(c * 2 + h) * blocks + i] for h in range(2)], axis=0)
             every = lax.dot_general(feat, ups[i], CONTRACT_MINOR, preferred_element_type=F32)
-            here = tokens[pl.ds(i, 1), :] - (sublane + float(c * span))
+            here = tokens[i : i + 1, :] - (sublane + float(c * span))
             sums = [None] * 4
             for g in range(span // 8):
                 term = jnp.where(here == float(8 * g), every[8 * g : 8 * g + 8, :], 0.0)
                 sums[g % 4] = term if sums[g % 4] is None else sums[g % 4] + term
             total = (sums[0] + sums[1]) + (sums[2] + sums[3])
-            dots[c, pl.ds(i, 1), :] = jnp.sum(total, axis=0, keepdims=True)
-
-        in_fours(b, one)
+            dots[c, i : i + 1, :] = jnp.sum(total, axis=0, keepdims=True)
+
+        for i in range(b * batch, (b + 1) * batch):
+            one(i)
         some = pl.ds(b * batch, batch)
-        for by in range(1, n_tp):
+        for by in far_first(n_tp):
             remote(
                 dots.at[c, some], dot_box.at[c, by, some], sent_sem.at[5], dot_sem.at[c * BATCHES + b], across(by)
             )
@@ -383,8 +386,8 @@
         coefs[c, low:high, :] = jax.nn.gelu(total) * shares[low:high, :]
 
         def one(i):
-            here = tokens[pl.ds(i, 1), :] - float(c * span) == token
-            coef = coefs[c, pl.ds(i, 1), :]
+            here = tokens[i : i + 1, :] - float(c * span) == token
+            coef = coefs[c, i : i + 1, :]
             coef_hi = coef.astype(BF16).astype(F32)
             spread = jnp.concatenate(
                 [jnp.where(here, x, 0.0).astype(BF16) for x in (coef_hi, coef - coef_hi)], axis=1
@@ -392,17 +395,18 @@
             both = jnp.concatenate([outs[i]] * 2, axis=0)
             parts[c, i] = jnp.dot(spread, both, preferred_element_type=F32)
 
-        in_fours(b, one)
-
-    share = 1.5 / CHUNKS
+        for i in range(b * batch, (b + 1) * batch):
+            one(i)
+
+    each = 0.66 / CHUNKS
     for c in range(CHUNKS):
         for b in range(BATCHES):
             mine_of = range(b * batch, (b + 1) * batch)
             needs = [("gather", i) for i in mine_of if i % GATHERS == 0]
             needs += [("pass", c, h, *order[i][:: 1 - 2 * h]) for i in mine_of for h in range(2)]
-            sends = [(("x",), 0.175 * batch, 5.0, ("totals", c, b))]
-            step(("dots", c, b), 0.1 + 0.055 * batch * share, needs, sends, functools.partial(take_dots, c, b))
-            step(("mix", c, b), 0.05 + 0.055 * batch * share, [("totals", c, b)], [], functools.partial(take_coefs, c, b))
+            sends = [(("x",), 0.175 * batch, ACROSS, ("totals", c, b))]
+            step(("dots", c, b), each, needs, sends, functools.partial(take_dots, c, b))
+            step(("mix", c, b), each, [("totals", c, b)], [], functools.partial(take_coefs, c, b))
 
     numbers = {}
 
@@ -446,8 +450,8 @@
             remote(outbox.at[here], ref, sent_sem.at[6], sem, along[axis](-way))
 
         needs = [("mix", c, place(h, q, p) // batch)] + [("sum", *key) for key in came]
-        sends = [((axis, -way), wire, hop, ("sum", *target))] if target else []
-        step(("add", c, h, q, p), 0.02 + 0.03 / CHUNKS, needs, sends, action)
+        sends = [((axis, -way), wire, HOP[axis, -way], ("sum", *target))] if target else []
+        step(("add", c, h, q, p), 0.045, needs, sends, action)
 
     for c in range(CHUNKS):
         for h in range(2):
@@ -461,7 +465,7 @@
         ones = jnp.ones((8, 2 * width), BF16)
         sums = lax.dot_general(ones, split, CONTRACT_MINOR, preferred_element_type=F32)
         squares[c, 0] = sums[:1]
-        for by in range(1, n_tp):
+        for by in far_first(n_tp):
             remote(squares.at[c, 0], squares.at[c, by], sent_sem.at[7], square_sem.at[c], across(by))
 
     def finish(c):
@@ -476,11 +480,21 @@
 
     for c in range(CHUNKS):
         needs = [("add", c, h, 0, 0) for h in range(2)]
-        step(("square", c), 0.2, needs, [(("x",), 0.4, 5.0, ("squares", c))], functools.partial(send_squares, c))
+        step(("square", c), 0.2, needs, [(("x",), 0.4, ACROSS, ("squares", c))], functools.partial(send_squares, c))
         step(("norm", c), 0.3, [("squares", c)], [], functools.partial(finish, c))
 
-    chunk_of = lambda name: name[1] if isinstance(name, tuple) and name[0] != "gather" else 0
-    plan = schedule(steps, SLACK, lambda name: LATER * chunk_of(name))
+    def late(name):
+        if isinstance(name, str):
+            return -5
+        kind, k = name[:2]
+        if kind in ("square", "norm"):
+            return -20
+        wait = -SOONER[kind, 0 if kind == "gather" else k]
+        if kind == "gather":
+            return wait + NEXT_BATCH * (k // batch)
+        return wait + NEXT_BATCH * name[2] * 0.5 if kind in ("dots", "mix") else wait
+
+    plan = schedule(steps, SLACK, late)
     with scope("barrier"):
         pl.semaphore_wait(barrier, len(peers))
     for name in plan:
@@ -536,7 +550,7 @@
             pltpu.VMEM((1, width), F32),
             pltpu.VMEM((2, held, width), BF16),
             pltpu.VMEM((2 * held, width), F32),
-            pltpu.VMEM((2 * cap, width), F32),
+            pltpu.VMEM((2, 2 * cap, width), F32),
             pltpu.VMEM((ring, ring, cap), I32),
             pltpu.VMEM((ring, ring, cap), I32),
             pltpu.VMEM((ring, ring, cap), I32),

time: 105 us -> 99 us (0.943)
  Pallas kernels: 104 us -> 98.2 us
    pallas_call x1, Pallas kernels: 101 us -> 95.7 us  [body(): pl.pallas_call(functools.partial(kernel, ring, n_tp), out_shape=jax.Shape...]
where the time goes in v5:
time: 99 us; the launch traced here: 98.8 us
  Pallas kernels  98.2 us (99%)
    pallas_call x1, Pallas kernels, body(): pl.pallas_call(functools.partial(kernel, ring, n_tp), out_shape=jax.Shape...  95.7 us
    pallas_call x1, Pallas kernels, body(): pl.pallas_call(functools.partial(bucket_kernel, held), out_shape=(jax.Sha...  2.51 us

profile of v5, /device:TPU:1, one launch (start us, length us, event | category | flops | bytes accessed | tf_op | source)
XLA Modules:
  0.0 98.8 jit_solution(3295208561259058115)
XLA Ops:
  0.0 2.5 %bucket.1 = (s32[8,8,128]{2,1,0:T(8,128)S(1)}, f32[8,8,128]{2,1,0:T(8,128)S(1)}, bf16[256,128]{1,0:T(8,128)(2,1)S(1)}) custom-call(s32[16,256]{1,0:T(8,128)} %bitcast.3, f32[16,256]{1,0:T(8,128)} %bitcast.4, bf16[256,128]{1,0:T(8,128)(2,1)} %token_hbm.1), custom_call_target="tpu_custom_call" | custom-call | tf_op jit(solution)/shard_map/bucket/pallas_call | solution.py:526
  2.5 95.7 %retrieve.1 = bf16[256,128]{1,0:T(8,128)(2,1)S(1)} custom-call(bf16[256,128]{1,0:T(8,128)(2,1)S(1)} %get-tuple-element.8.refs_0_, s32[8,8,128]{2,1,0:T(8,128)S(1)} %get-tuple-element.9.refs_1_, f32[8,8,128]{2,1,0:T(8,128)S(1)} %get-tuple-element.10.refs_2_, bf16[4096,128]{1,0:T(8,128)(2,1)} %refs_3_.1, bf16[4096,128]{1,0:T(8,128)(2,1)} %refs_4_.1, ...), custom_call_target="tpu_custom_call" | custom-call | tf_op jit(solution)/shard_map/retrieve/pallas_call | solution.py:543
  98.2 0.6 copy.8

commit v6 on v5

--- a/solution.py
+++ b/solution.py
@@ -413,18 +413,24 @@
     def box(*key):
         sem = sum_sem.at[numbers.setdefault(key, len(numbers))]
         kind, c, h, q, p, way = key
+        if kind == 3:
+            return inbox2.at[(c * 2 + h) * (ring + 3) + ring + (1 if q < ring // 2 else 2)], sem
         if kind == 1:
             if p == 0 and way < 0:
                 return inbox_x.at[(c * 2 + h) * ring + q], sem
             return inbox.at[slot(c, h, q, p)], sem
-        return inbox2.at[(c * 2 + h) * (ring + 1) + (ring if q == 0 and way < 0 else q)], sem
+        return inbox2.at[(c * 2 + h) * (ring + 3) + (ring if q == 0 and way < 0 else q)], sem
 
     def add_up(c, h, q, p):
         here = slot(c, h, q, p)
         plus = q % 2 == 0
         came = [(1, c, h, q, p, way if p == 0 else 0) for way in beyond(ring, p, plus)]
-        if p == 0:
+        straight = c == CHUNKS - 1
+        far = 1
+        if p == 0 and not (straight and distance(ring, q) == 1):
             came += [(2, c, h, q, 0, way if q == 0 else 0) for way in beyond(ring, q, h == 0)]
+        if straight and (q, p) == (0, 0):
+            came += [(3, c, h, k, 0, 0) for k in (2, ring - 2)]
         if p:
             way, axis = heading(ring, p, plus), 1 - h
             after = (p - way) % ring
@@ -433,6 +439,8 @@
             way, axis = heading(ring, q, h == 0), h
             after = (q - way) % ring
             target = (2, c, h, after, 0, way if after == 0 else 0)
+            if straight and distance(ring, q) == 2:
+                target, far = (3, c, h, q, 0, 0), 2
         else:
             target = None
 
@@ -447,10 +455,10 @@
                 return
             outbox[here] = value.astype(BF16)
             ref, sem = box(*target)
-            remote(outbox.at[here], ref, sent_sem.at[6], sem, along[axis](-way))
+            remote(outbox.at[here], ref, sent_sem.at[6], sem, along[axis](-way * far))
 
         needs = [("mix", c, place(h, q, p) // batch)] + [("sum", *key) for key in came]
-        sends = [((axis, -way), wire, HOP[axis, -way], ("sum", *target))] if target else []
+        sends = [((axis, -way), wire * far, HOP[axis, -way] + 0.75 * (far - 1), ("sum", *target))] if target else []
         step(("add", c, h, q, p), 0.045, needs, sends, action)
 
     for c in range(CHUNKS):
@@ -570,7 +578,7 @@
             pltpu.VMEM((CHUNKS, n_ep, 2 * rows, width), F32),
             pltpu.VMEM((blocks, rows, width), BF16),
             pltpu.VMEM((2 * CHUNKS * ring, rows, width), BF16),
-            pltpu.VMEM((2 * CHUNKS * (ring + 1), rows, width), BF16),
+            pltpu.VMEM((2 * CHUNKS * (ring + 3), rows, width), BF16),
             pltpu.VMEM((blocks, rows, width), BF16),
             pltpu.VMEM((CHUNKS, 2 * rows, width), F32),
             pltpu.VMEM((CHUNKS, n_tp, 1, 2 * rows), F32),

time: 99 us -> 97.6 us (0.986)
  Pallas kernels: 98.2 us -> 96.8 us
    pallas_call x1, Pallas kernels: 95.7 us -> 94.3 us  [body(): pl.pallas_call(functools.partial(kernel, ring, n_tp), out_shape=jax.Shape...]
where the time goes in v6:
time: 97.6 us; the launch traced here: 97.5 us
  Pallas kernels  96.8 us (99%)
    pallas_call x1, Pallas kernels, body(): pl.pallas_call(functools.partial(kernel, ring, n_tp), out_shape=jax.Shape...  94.3 us
    pallas_call x1, Pallas kernels, body(): pl.pallas_call(functools.partial(bucket_kernel, held), out_shape=(jax.Sha...  2.51 us

profile of v6, /device:TPU:1, one launch (start us, length us, event | category | flops | bytes accessed | tf_op | source)
XLA Modules:
  0.0 97.5 jit_solution(8016939092839963382)
XLA Ops:
  0.0 2.5 %bucket.1 = (s32[8,8,128]{2,1,0:T(8,128)S(1)}, f32[8,8,128]{2,1,0:T(8,128)S(1)}, bf16[256,128]{1,0:T(8,128)(2,1)S(1)}) custom-call(s32[16,256]{1,0:T(8,128)} %bitcast.3, f32[16,256]{1,0:T(8,128)} %bitcast.4, bf16[256,128]{1,0:T(8,128)(2,1)} %token_hbm.1), custom_call_target="tpu_custom_call" | custom-call | tf_op jit(solution)/shard_map/bucket/pallas_call | solution.py:534
  2.5 94.3 %retrieve.1 = bf16[256,128]{1,0:T(8,128)(2,1)S(1)} custom-call(bf16[256,128]{1,0:T(8,128)(2,1)S(1)} %get-tuple-element.8.refs_0_, s32[8,8,128]{2,1,0:T(8,128)S(1)} %get-tuple-element.9.refs_1_, f32[8,8,128]{2,1,0:T(8,128)S(1)} %get-tuple-element.10.refs_2_, bf16[4096,128]{1,0:T(8,128)(2,1)} %refs_3_.1, bf16[4096,128]{1,0:T(8,128)(2,1)} %refs_4_.1, ...), custom_call_target="tpu_custom_call" | custom-call | tf_op jit(solution)/shard_map/retrieve/pallas_call | solution.py:551
  96.8 0.6 copy.8
